TPU v7x, 32 devices: a whole 2x2x4 slice. The times are simulated.
32 devices in a mesh: ep: 8 (over z, y), tp: 4 (over x, core).
Axes of the slice: x: 2, y: 2, z: 4, core: 2. Of those that a mesh axis runs over, the one named last changes fastest.
Arguments:
- tokens: bfloat16 [384, 2048], P(('ep', 'tp')), may hold values from -6 to 6
- cache_latent: bfloat16 [384, 1024, 512], P(('ep', 'tp')), may hold values from -1700 to 1700
- cache_rope: bfloat16 [384, 64, 1024], P(('ep', 'tp')), may hold values from -6 to 6
- lengths: int32 [384], P(('ep', 'tp')), may hold values from 128 to 1023, as said below
- attn_gain: bfloat16 [2048], replicated, may hold values from 0.099609375 to 1.8984375
- latent_gain: bfloat16 [512], replicated, may hold values from 0.099609375 to 1.8984375
- post_attn_gain: bfloat16 [2048], replicated, may hold values from 0.099609375 to 1.8984375
- ffn_gain: bfloat16 [2048], replicated, may hold values from 0.099609375 to 1.8984375
- post_ffn_gain: bfloat16 [2048], replicated, may hold values from 0.099609375 to 1.8984375
- w_query: bfloat16 [2048, 2048], P(None, 'tp'), may hold values from -0.125 to 0.125
- w_query_rot: bfloat16 [2048, 1024], P(None, 'tp'), may hold values from -0.125 to 0.125
- w_latent: bfloat16 [2048, 512], P(None, 'tp'), may hold values from -0.125 to 0.125
- w_key_rot: bfloat16 [2048, 64], replicated, may hold values from -0.125 to 0.125
- w_key_up: bfloat16 [512, 16, 128], P(None, 'tp'), may hold values from -0.25 to 0.25
- w_value_up: bfloat16 [512, 16, 128], P(None, 'tp'), may hold values from -0.25 to 0.25
- w_out: bfloat16 [2048, 2048], P('tp'), may hold values from -0.125 to 0.125
- route_logits: float32 [384, 4], P('ep'), may hold values from -6 to 6
- routes: int32 [384, 4], P('ep'), may hold values from 0 to 7, all different within a row; in each aligned block of 48 rows (0 to 47, 48 to 95, ...) at most 25 rows name the same one
- w_gate: bfloat16 [8, 2048, 2048], P('ep', None, 'tp'), may hold values from -0.3125 to 0.3125
- w_up: bfloat16 [8, 2048, 2048], P('ep', None, 'tp'), may hold values from -0.3125 to 0.3125
- w_down: bfloat16 [8, 2048, 2048], P('ep', 'tp'), may hold values from -0.125 to 0.125
Outputs:
- result: bfloat16 [384, 2048], P(('ep', 'tp'))
- new_latent: bfloat16 [384, 512], P(('ep', 'tp'))
- new_rope: bfloat16 [384, 64], P(('ep', 'tp'))
Inputs may be any that keep to these rules, and one draw needn't show every extreme that they name: Each sequence's cache holds positions 0 to lengths - 1, and the new token stands at position lengths; some sequence has 1023 in every draw. `routes`: each row names 4 different experts; in each aligned block of 48 rows (the tokens of one index of ep) no expert is named more than 25 times, a bound that some block reaches.
All inputs are finite; a program needn't handle non-finite values.
Results may differ from a plain program's by a relative error of at most 0.019.
Values may be sent and summed in bfloat16 or wider, within the bound.
A program may use at most 128 MiB of HBM per device.

v0:
```python
import functools

import jax
import jax.numpy as jnp
import numpy as np
from jax import lax
from jax.experimental import pallas as pl
from jax.experimental.pallas import tpu as pltpu
from jax.sharding import PartitionSpec as P

eps_norm = 1e-06
clamp_limit = 7.0
sigmoid_alpha = 1.702
theta_base = 10000.0
MESH = pl.DeviceIdType.MESH
F32 = jnp.float32
BF16 = jnp.bfloat16


def rms_scale(values, gain):
    mean_square = jnp.mean(values * values, axis=-1, keepdims=True)
    return values * lax.rsqrt(mean_square + eps_norm) * gain


def turn(values, cosine, sine):
    half = values.shape[-1] // 2
    swapped = jnp.concatenate([values[:, half:], values[:, :half]], axis=1)
    return values * cosine + swapped * sine


def dot(a, b):
    return jnp.dot(a, b, preferred_element_type=F32)


def dot_nt(a, b):
    return lax.dot_general(a, b, (((1,), (1,)), ((), ())), preferred_element_type=F32)


def remote(src, dst, send_sem, recv_sem, where):
    return pltpu.make_async_remote_copy(
        src_ref=src,
        dst_ref=dst,
        send_sem=send_sem,
        recv_sem=recv_sem,
        device_id=where,
        device_id_type=MESH,
    )


def kernel(
    cfg,
    lengths,
    tokens,
    attn_gain,
    latent_gain,
    post_attn_gain,
    ffn_gain,
    post_ffn_gain,
    routes_t,
    logits_t,
    cache_h,
    rope_h,
    wq_h,
    wqr_h,
    wl_h,
    wkr_h,
    wku_h,
    wvu_h,
    wo_h,
    wg_h,
    wu_h,
    wd_h,
    out_result,
    out_latent,
    out_rope,
    cache,
    rope,
    wq,
    wqr,
    wl,
    wkr,
    wku,
    wvu,
    wo,
    wg,
    wu,
    wd,
    xg,
    qsend,
    qrecv,
    qs,
    qt,
    nlat,
    nrope,
    hl,
    hsend,
    hrecv,
    asend,
    arecv,
    fg,
    sl,
    xr,
    act,
    part,
    s1,
    xsend,
    xrecv,
    rsend,
    ret,
    msend,
    mrecv,
    ku3,
    vu3,
    wide,
    sc,
    pb,
    w_sem,
    c_sem,
    r_sem,
    tp_send,
    tp_recv,
    own_sem,
    d_send,
    d_recv,
    x_send,
    x_recv,
    sib_send,
    sib_recv,
    s1_send,
    s1_recv,
    rx_send,
    rx_recv,
    ret_send,
    ret_recv,
):
    T, EP, R, RP, LH, CP, scale = cfg
    H = T * LH
    t = lax.axis_index("tp")
    e = lax.axis_index("ep")
    C = wku.shape[0]
    KD = wq.shape[1] // LH
    RD = wkr.shape[0]
    VD = wvu.shape[1] // LH
    LC = wl.shape[1]
    D = wq.shape[0]
    Q = D // T
    G = T * RP
    S = EP * CP
    SPAN = cache.shape[1]
    sib = t + 1 - 2 * lax.rem(t, 2)

    loads = {}
    for i, (name, src, dst) in enumerate(
        [
            ("wq", wq_h, wq),
            ("wqr", wqr_h, wqr),
            ("wl", wl_h, wl),
            ("wkr", wkr_h, wkr),
            ("wku", wku_h, ku3),
            ("wvu", wvu_h, vu3),
            ("wo", wo_h, wo),
            ("wg", wg_h.at[0], wg),
            ("wu", wu_h.at[0], wu),
            ("wd", wd_h.at[0], wd),
        ]
    ):
        loads[name] = pltpu.make_async_copy(src, dst, w_sem.at[i])
    for name in ("wku", "wkr", "wq", "wqr", "wl"):
        loads[name].start()

    barrier = pltpu.get_barrier_semaphore()
    for k in range(1, T):
        pl.semaphore_signal(
            barrier, inc=1, device_id={"tp": lax.rem(t + k, T)}, device_id_type=MESH
        )
    for k in range(1, EP):
        pl.semaphore_signal(
            barrier, inc=1, device_id={"ep": lax.rem(e + k, EP)}, device_id_type=MESH
        )

    def cache_copy(b):
        return pltpu.make_async_copy(cache_h.at[b], cache.at[b], c_sem.at[b])

    def rope_copy(b):
        return pltpu.make_async_copy(rope_h.at[b], rope.at[b], r_sem.at[b])

    def gain(ref):
        return ref[...].astype(F32)[None, :]

    def by_head_columns(source, target):
        size = source.shape[2]
        wide[...] = source[...].astype(F32).reshape(C * LH, size)
        for h in range(LH):
            target[:, h * size : (h + 1) * size] = wide[pl.ds(h, C, stride=LH), :].astype(BF16)

    token_values = jnp.concatenate(
        [tokens[...].astype(F32), jnp.zeros((RP - R, D), F32)], axis=0
    )
    xg[t] = rms_scale(token_values, gain(attn_gain)).astype(BF16)
    pl.semaphore_wait(barrier, T - 1 + EP - 1)

    def gather_tp(phase, buf):
        copies = []
        for k in range(1, T):
            c = remote(
                buf.at[t],
                buf.at[t],
                tp_send.at[phase, k],
                tp_recv.at[phase, k],
                {"tp": lax.rem(t + k, T)},
            )
            c.start()
            copies.append(c)
        return copies

    def scatter_tp(phase, src, dst):
        copies = []
        for k in range(1, T):
            peer = lax.rem(t + k, T)
            c = remote(
                src.at[peer],
                dst.at[t],
                tp_send.at[phase, k],
                tp_recv.at[phase, k],
                {"tp": peer},
            )
            c.start()
            copies.append(c)
        dst[t] = src[t]
        return copies

    def finish(copies):
        for c in copies:
            c.wait()

    copies = gather_tp(0, xg)
    for b in range(R):
        cache_copy(b).start()
        rope_copy(b).start()
    loads["wku"].wait()
    by_head_columns(ku3, wku)
    half = RD // 2
    lane = lax.broadcasted_iota(jnp.int32, (RP, RD), 1)
    row = lax.broadcasted_iota(jnp.int32, (RP, RD), 0)
    freqs = jnp.zeros((RP, RD), F32)
    for i in range(half):
        hit = (lane == i) | (lane == i + half)
        freqs = jnp.where(hit, np.float32(theta_base ** (-i / half)), freqs)
    positions = jnp.zeros((RP, RD), jnp.int32)
    for b in range(R):
        positions = jnp.where(row == b, lengths[b], positions)
    angles = positions.astype(F32) * freqs
    cosine = jnp.cos(angles)
    sine = jnp.sin(angles)
    sine = jnp.where(lane < half, -sine, sine)
    loads["wkr"].wait()
    key_raw = dot_nt(xg[t], wkr[...]).astype(BF16).astype(F32)
    new_rope = turn(key_raw, cosine, sine).astype(BF16)
    nrope[...] = new_rope.astype(F32)
    out_rope[...] = new_rope[:R]
    for name in ("wq", "wqr", "wl"):
        loads[name].wait()
    finish(copies)

    rows = xg[...].reshape(G, D)
    plain = dot(rows, wq[...]).astype(BF16)
    rotary = dot(rows, wqr[...]).astype(BF16)
    latent_part = dot(rows, wl[...]).astype(BF16)
    for h in range(LH):
        lat = dot_nt(plain[:, h * KD : (h + 1) * KD], wku[:, h * KD : (h + 1) * KD])
        qsend[:, :, h * C : (h + 1) * C] = lat.astype(BF16).reshape(T, RP, C)
    base = LH * C
    qsend[:, :, base : base + LH * RD] = rotary.reshape(T, RP, LH * RD)
    qsend[:, :, base + LH * RD :] = latent_part.reshape(T, RP, LC)
    copies = scatter_tp(1, qsend, qrecv)
    for name in ("wvu", "wo", "wg", "wu", "wd"):
        loads[name].start()
    ri = lax.broadcasted_iota(jnp.int32, (RP * H, RP * H), 0)
    ci = lax.broadcasted_iota(jnp.int32, (RP * H, RP * H), 1)
    head_shift = H.bit_length() - 1
    row_shift = RP.bit_length() - 1
    to_seq = (
        ci == ((ri & (H - 1)) << row_shift) + (ri >> head_shift)
    ).astype(F32).astype(BF16)
    to_head = (
        ci == ((ri & (RP - 1)) << head_shift) + (ri >> row_shift)
    ).astype(F32).astype(BF16)
    finish(copies)

    latent_raw = jnp.concatenate(
        [qrecv[s, :, base + LH * RD :] for s in range(T)], axis=1
    ).astype(F32)
    new_latent = rms_scale(latent_raw, gain(latent_gain)).astype(BF16)
    out_latent[...] = new_latent[:R]
    nlat[...] = new_latent.astype(F32)
    stacked = jnp.concatenate(
        [qrecv[s, :, h * C : (h + 1) * C] for s in range(T) for h in range(LH)], axis=0
    )
    qs[...] = dot(to_seq, stacked).astype(BF16).reshape(RP, H, C)
    turned = jnp.concatenate(
        [
            turn(
                qrecv[s, :, base + h * RD : base + (h + 1) * RD].astype(F32),
                cosine,
                sine,
            ).astype(BF16)
            for s in range(T)
            for h in range(LH)
        ],
        axis=0,
    )
    qt[...] = dot(to_seq, turned).astype(BF16).reshape(RP, H, RD)
    if RP > R:
        hl[R:] = jnp.zeros((RP - R, H, C), BF16)

    position = lax.broadcasted_iota(jnp.int32, (H, SPAN), 1)
    for b in range(R):
        cache_copy(b).wait()
        rope_copy(b).wait()
        scores = (dot_nt(qs[b], cache[b]) + dot(qt[b], rope[b])) * scale
        sc[b] = jnp.where(position < lengths[b], scores, -jnp.inf)
    prob_own = []
    for b in range(R):
        own = (
            jnp.sum(qs[b].astype(F32) * nlat[b : b + 1, :], axis=1, keepdims=True)
            + jnp.sum(qt[b].astype(F32) * nrope[b : b + 1, :], axis=1, keepdims=True)
        ) * scale
        masked = sc[b]
        highest = jnp.maximum(jnp.max(masked, axis=1, keepdims=True), own)
        raised = jnp.exp(masked - highest)
        raised_own = jnp.exp(own - highest)
        inverse = 1.0 / (jnp.sum(raised, axis=1, keepdims=True) + raised_own)
        pb[b] = (raised * inverse).astype(BF16)
        prob_own.append((raised_own * inverse).astype(BF16).astype(F32))
    for b in range(R):
        hl[b] = (dot(pb[b], cache[b]) + prob_own[b] * nlat[b : b + 1, :]).astype(BF16)

    by_head = dot(to_head, hl[...].reshape(RP * H, C)).astype(BF16)
    hsend[...] = by_head.reshape(T, LH * RP, C)
    copies = scatter_tp(2, hsend, hrecv)
    loads["wvu"].wait()
    by_head_columns(vu3, wvu)
    loads["wo"].wait()

    N = routes_t.shape[1]
    slot_shift = CP.bit_length() - 1
    s_sub = lax.broadcasted_iota(jnp.int32, (S, N), 0)
    e_sub = s_sub >> slot_shift
    c_sub = (s_sub & (CP - 1)).astype(F32)
    gi = lax.broadcasted_iota(jnp.int32, (N, N), 0)
    gj = lax.broadcasted_iota(jnp.int32, (N, N), 1)
    upper = (gi < gj).astype(F32).astype(BF16)
    pi = lax.broadcasted_iota(jnp.int32, (G, N), 0)
    pj = lax.broadcasted_iota(jnp.int32, (G, N), 1)
    spread = jnp.zeros((G, N), F32)
    for s in range(T):
        inside = (pj >= s * R) & (pj < (s + 1) * R)
        spread = jnp.where(inside & (pi == pj + s * (RP - R)), 1.0, spread)
    spread = spread.astype(BF16)
    lg = logits_t[...]
    lg = jnp.exp(lg - jnp.max(lg, axis=0, keepdims=True))
    weights = lg / jnp.sum(lg, axis=0, keepdims=True)
    count = jnp.zeros((S, N), F32)
    weighted = jnp.zeros((S, N), F32)
    for k in range(routes_t.shape[0]):
        hit = routes_t[k : k + 1, :] == e_sub
        count = jnp.where(hit, 1.0, count)
        weighted = jnp.where(hit, weights[k : k + 1, :], weighted)
    rank = dot(count.astype(BF16), upper)
    taken = rank == c_sub
    weighted = jnp.where(taken, weighted, 0.0)
    weighted_hi = weighted.astype(BF16)
    weighted_lo = (weighted - weighted_hi.astype(F32)).astype(BF16)
    combine_hi = dot_nt(spread, weighted_hi).astype(BF16)
    combine_lo = dot_nt(spread, weighted_lo).astype(BF16)
    dispatch = dot_nt(jnp.where(taken, count, 0.0).astype(BF16), spread).astype(BF16)

    finish(copies)
    values = []
    for h in range(LH):
        mine = jnp.concatenate(
            [hrecv[s, h * RP : (h + 1) * RP, :] for s in range(T)], axis=0
        )
        values.append(dot(mine, wvu[:, h * VD : (h + 1) * VD]).astype(BF16))
    values = jnp.concatenate(values, axis=1)
    asend[...] = dot(values, wo[...]).astype(BF16).reshape(T, RP, D)
    finish(scatter_tp(3, asend, arecv))
    attn = arecv[0].astype(F32)
    for s in range(1, T):
        attn = attn + arecv[s].astype(F32)
    attn = attn.astype(BF16).astype(F32)
    mixed = (token_values + rms_scale(attn, gain(post_attn_gain))).astype(BF16).astype(F32)
    fg[t] = rms_scale(mixed, gain(ffn_gain)).astype(BF16)
    finish(gather_tp(4, fg))

    mine = fg[:, :, pl.ds(pl.multiple_of(t * Q, Q), Q)].reshape(G, Q)
    sl[...] = dot(dispatch, mine).astype(BF16).reshape(EP, CP, Q)
    sent = [None]
    for k in range(1, EP):
        peer = lax.rem(e + k, EP)
        c = remote(sl.at[peer], xr.at[t, e], d_send.at[k], d_recv.at[k], {"ep": peer})
        c.start()
        sent.append(c)
    xr[t, e] = sl[e]
    pairs = T // 2
    across = []
    to_sib = []
    for k in range(EP):
        src = lax.rem(e + EP - k, EP)
        if k:
            sent[k].wait_recv()
        row = []
        for j in range(1, pairs):
            c = remote(
                xr.at[t, src],
                xr.at[t, src],
                x_send.at[k, j],
                x_recv.at[k, j],
                {"tp": lax.rem(t + 2 * j, T)},
            )
            c.start()
            row.append(c)
        across.append(row)
        c = remote(
            xr.at[t, src], xr.at[t, src], sib_send.at[k, 0], sib_recv.at[k, 0], {"tp": sib}
        )
        c.start()
        to_sib.append(c)
    for k in range(EP):
        src = lax.rem(e + EP - k, EP)
        for j in range(1, pairs):
            across[k][j - 1].wait_recv()
            quarter = lax.rem(t + T - 2 * j, T)
            c = remote(
                xr.at[quarter, src],
                xr.at[quarter, src],
                sib_send.at[k, j],
                sib_recv.at[k, j],
                {"tp": sib},
            )
            c.start()
            to_sib.append(c)
    for name in ("wg", "wu", "wd"):
        loads[name].wait()
    for c in to_sib:
        c.wait_recv()

    gate = jnp.zeros((S, wg.shape[1]), F32)
    upward = jnp.zeros((S, wg.shape[1]), F32)
    for q in range(T):
        block = xr[q].reshape(S, Q)
        gate = gate + dot(block, wg[q * Q : (q + 1) * Q, :])
        upward = upward + dot(block, wu[q * Q : (q + 1) * Q, :])
    gate = jnp.minimum(gate, clamp_limit)
    upward = jnp.clip(upward, -clamp_limit, clamp_limit)
    active = (upward + 1.0) * gate * (1.0 / (1.0 + jnp.exp(-sigmoid_alpha * gate)))
    act[...] = active.astype(BF16)

    halves = []
    for j in range(pairs - 1, -1, -1):
        quarter = lax.rem(sib + 2 * j, T)
        cols = pl.ds(pl.multiple_of(quarter * Q, Q), Q)
        part[quarter] = dot(act[...], wd[:, cols]).astype(BF16).reshape(EP, CP, Q)
        c = remote(
            part.at[quarter], s1.at[quarter], s1_send.at[j], s1_recv.at[j], {"tp": sib}
        )
        c.start()
        halves.append((j, c))
    for j in range(pairs - 1, -1, -1):
        quarter = lax.rem(t + 2 * j, T)
        cols = pl.ds(pl.multiple_of(quarter * Q, Q), Q)
        part[quarter] = dot(act[...], wd[:, cols]).astype(BF16).reshape(EP, CP, Q)
    reduced = [[None] * pairs for _ in range(EP)]
    order = list(range(1, EP)) + [0]
    for j, c in halves:
        c.wait_recv()
        if j == 0:
            continue
        quarter = lax.rem(t + 2 * j, T)
        for k in order:
            src = lax.rem(e + EP - k, EP)
            both = part[quarter, src].astype(F32) + s1[quarter, src].astype(F32)
            xsend[j, src] = both.astype(BF16)
            cc = remote(
                xsend.at[j, src],
                xrecv.at[j, src],
                rx_send.at[k, j],
                rx_recv.at[k, j],
                {"tp": quarter},
            )
            cc.start()
            reduced[k][j] = cc
    back = []
    for k in order:
        src = lax.rem(e + EP - k, EP)
        total = part[t, src].astype(F32) + s1[t, src].astype(F32)
        for j in range(1, pairs):
            reduced[k][j].wait_recv()
            total = total + xrecv[j, src].astype(F32)
        if k:
            rsend[src] = total.astype(BF16)
            c = remote(rsend.at[src], ret.at[e], ret_send.at[k], ret_recv.at[k], {"ep": src})
            c.start()
            back.append(c)
        else:
            ret[e] = total.astype(BF16)
    for c in back:
        c.wait_recv()
    returned = ret[...].reshape(S, Q)
    moe_part = dot(combine_hi, returned) + dot(combine_lo, returned)
    msend[...] = moe_part.astype(BF16).reshape(T, RP, Q)
    finish(scatter_tp(5, msend, mrecv))
    moe = jnp.concatenate([mrecv[s] for s in range(T)], axis=1).astype(F32)
    out_result[...] = (mixed + rms_scale(moe, gain(post_ffn_gain))).astype(BF16)[:R]

    for c in sent[1:] + to_sib + [c for row in across for c in row] + back:
        c.wait_send()
    for _, c in halves:
        c.wait_send()
    for row in reduced:
        for c in row[1:]:
            c.wait_send()


def hand_over(result, latent, rope, out_result, out_latent, out_rope):
    out_result[...] = result[...]
    out_latent[...] = latent[...]
    out_rope[...] = rope[...]


def body(
    tokens,
    cache_latent,
    cache_rope,
    lengths,
    attn_gain,
    latent_gain,
    post_attn_gain,
    ffn_gain,
    post_ffn_gain,
    w_query,
    w_query_rot,
    w_latent,
    w_key_rot,
    w_key_up,
    w_value_up,
    w_out,
    route_logits,
    routes,
    w_gate,
    w_up,
    w_down,
):
    R, D = tokens.shape
    T = lax.axis_size("tp")
    EP = lax.axis_size("ep")
    C, LH, KD = w_key_up.shape
    RD = w_key_rot.shape[1]
    VD = w_value_up.shape[2]
    H = T * LH
    K = routes.shape[1]
    scale = (KD + RD) ** (-0.5)
    RP = 16
    while RP < R:
        RP *= 2
    cap = (R * T * K + EP - 1) // EP + 1
    CP = 16
    while CP < cap:
        CP *= 2
    Q = D // T
    F = w_gate.shape[2]
    LC = w_latent.shape[1]
    SPAN = cache_latent.shape[1]

    vm = pl.BlockSpec(memory_space=pltpu.VMEM)
    hbm = pl.BlockSpec(memory_space=pl.ANY)
    dma = pltpu.SemaphoreType.DMA
    pairs = T // 2
    QW = LH * C + LH * RD + LC

    def v(*shape, dtype=BF16):
        return pltpu.VMEM(shape, dtype)

    cfg = (T, EP, R, RP, LH, CP, scale)
    outs = pl.pallas_call(
        functools.partial(kernel, cfg),
        out_shape=(
            jax.ShapeDtypeStruct((R, D), BF16),
            jax.ShapeDtypeStruct((R, C), BF16),
            jax.ShapeDtypeStruct((R, RD), BF16),
        ),
        in_specs=[pl.BlockSpec(memory_space=pltpu.SMEM)] + [vm] * 8 + [hbm] * 12,
        out_specs=(vm, vm, vm),
        scratch_shapes=[
            v(R, SPAN, C),
            v(R, RD, SPAN),
            v(D, LH * KD),
            v(D, LH * RD),
            v(D, LC),
            v(RD, D),
            v(C, LH * KD),
            v(C, LH * VD),
            v(LH * VD, D),
            v(D, F),
            v(D, F),
            v(F, D),
            v(T, RP, D),
            v(T, RP, QW),
            v(T, RP, QW),
            v(RP, H, C),
            v(RP, H, RD),
            v(RP, C, dtype=F32),
            v(RP, RD, dtype=F32),
            v(RP, H, C),
            v(T, LH * RP, C),
            v(T, LH * RP, C),
            v(T, RP, D),
            v(T, RP, D),
            v(T, RP, D),
            v(EP, CP, Q),
            v(T, EP, CP, Q),
            v(EP * CP, F),
            v(T, EP, CP, Q),
            v(T, EP, CP, Q),
            v(pairs, EP, CP, Q),
            v(pairs, EP, CP, Q),
            v(EP, CP, Q),
            v(EP, CP, Q),
            v(T, RP, Q),
            v(T, RP, Q),
            v(C, LH, KD),
            v(C, LH, VD),
            v(C * LH, KD, dtype=F32),
            v(R, H, SPAN, dtype=F32),
            v(R, H, SPAN),
            dma((10,)),
            dma((R,)),
            dma((R,)),
            dma((6, T)),
            dma((6, T)),
            dma((1,)),
            dma((EP,)),
            dma((EP,)),
            dma((EP, pairs)),
            dma((EP, pairs)),
            dma((EP, pairs)),
            dma((EP, pairs)),
            dma((pairs,)),
            dma((pairs,)),
            dma((EP, pairs)),
            dma((EP, pairs)),
            dma((EP,)),
            dma((EP,)),
        ],
        compiler_params=pltpu.CompilerParams(
            collective_id=0, has_side_effects=True, vmem_limit_bytes=60 * 1024 * 1024
        ),
    )(
        lengths,
        tokens,
        attn_gain,
        latent_gain,
        post_attn_gain,
        ffn_gain,
        post_ffn_gain,
        routes.T,
        route_logits.T,
        cache_latent,
        cache_rope,
        w_query,
        w_query_rot,
        w_latent,
        w_key_rot.T,
        w_key_up,
        w_value_up,
        w_out,
        w_gate,
        w_up,
        w_down,
    )
    return pl.pallas_call(
        hand_over,
        out_shape=tuple(jax.ShapeDtypeStruct(o.shape, o.dtype) for o in outs),
        in_specs=[vm] * 3,
        out_specs=(vm, vm, vm),
    )(*outs)


def solution(mesh):
    return jax.shard_map(
        body,
        mesh=mesh,
        in_specs=(
            P(("ep", "tp"), None),
            P(("ep", "tp"), None, None),
            P(("ep", "tp"), None, None),
            P(("ep", "tp")),
            P(),
            P(),
            P(),
            P(),
            P(),
            P(None, "tp"),
            P(None, "tp"),
            P(None, "tp"),
            P(),
            P(None, "tp", None),
            P(None, "tp", None),
            P("tp", None),
            P("ep", None),
            P("ep", None),
            P("ep", None, "tp"),
            P("ep", None, "tp"),
            P("ep", "tp", None),
        ),
        out_specs=(P(("ep", "tp"), None), P(("ep", "tp"), None), P(("ep", "tp"), None)),
        check_vma=False,
    )
```

profile of v0, /device:TPU:0, one launch (start us, length us, event | category | flops | bytes accessed | tf_op | source)
XLA Modules:
  0.0 76.0 jit_solution(3909874431465672118)
XLA Ops:
  0.6 73.9 %shard_map.220 = (bf16[12,2048]{1,0:T(8,128)(2,1)}, bf16[12,512]{1,0:T(8,128)(2,1)}, bf16[12,64]{1,0:T(8,128)(2,1)}) custom-call(s32[12]{0:T(128)} %lengths.1, bf16[12,2048]{1,0:T(8,128)(2,1)} %tokens.1, bf16[2048]{0:T(1024)(128)(2,1)} %attn_gain.1, bf16[512]{0:T(512)(128)(2,1)} %latent_gain.1, bf16[2048]{0:T(1024)(128)(2,1)} %post_attn_gain.1, ...), custom_call_target="tpu_custom_call" | custom-call | tf_op jit(solution)/shard_map/pallas_call | solution.py:585
  74.5 1.5 %shard_map.221 = (bf16[12,2048]{1,0:T(8,128)(2,1)}, bf16[12,512]{1,0:T(8,128)(2,1)}, bf16[12,64]{1,0:T(8,128)(2,1)}) custom-call(bf16[12,2048]{1,0:T(8,128)(2,1)} %get-tuple-element.6.result, bf16[12,512]{1,0:T(8,128)(2,1)} %get-tuple-element.7.latent, bf16[12,64]{1,0:T(8,128)(2,1)} %get-tuple-element.8.rope), custom_call_target="tpu_custom_call" | custom-call | tf_op jit(solution)/shard_map/pallas_call | solution.py:681
where the time goes:
time: 76.2 us; the launch traced here: 76 us
  Pallas kernels  75.4 us (99%)
    pallas_call x1, Pallas kernels, body(): pl.pallas_call(functools.partial(kernel, cfg), out_shape=(jax.ShapeDtypeS...  73.9 us

commit v1 on v0

v1 whole, which is shorter than its diff:
```python
import functools

import jax
import jax.numpy as jnp
import numpy as np
from jax import lax
from jax.experimental import pallas as pl
from jax.experimental.pallas import tpu as pltpu
from jax.sharding import PartitionSpec as P

eps_norm = 1e-06
clamp_limit = 7.0
sigmoid_alpha = 1.702
theta_base = 10000.0
MESH = pl.DeviceIdType.MESH
F32 = jnp.float32
BF16 = jnp.bfloat16
SUB = 8
LANES = 128


def rms_scale(values, gain):
    mean_square = jnp.mean(values * values, axis=-1, keepdims=True)
    return values * lax.rsqrt(mean_square + eps_norm) * gain


def turn(values, cosine, sine):
    half = values.shape[-1] // 2
    swapped = jnp.concatenate([values[:, half:], values[:, :half]], axis=1)
    return values * cosine + swapped * sine


def dot(a, b):
    return jnp.dot(a, b, preferred_element_type=F32)


def dot_nt(a, b):
    return lax.dot_general(a, b, (((1,), (1,)), ((), ())), preferred_element_type=F32)


def remote(src, dst, send_sem, recv_sem, where):
    return pltpu.make_async_remote_copy(
        src_ref=src,
        dst_ref=dst,
        send_sem=send_sem,
        recv_sem=recv_sem,
        device_id=where,
        device_id_type=MESH,
    )


def half_rows(values):
    return lax.broadcasted_iota(jnp.int32, values.shape, 0) < SUB // 2


def join_halves(upper, lower):
    return jnp.where(half_rows(upper), upper, pltpu.roll(lower, SUB // 2, 0))


def join_ends(upper, lower):
    return jnp.where(half_rows(upper), pltpu.roll(upper, SUB // 2, 0), lower)


def layout(T, R, LH):
    H = T * LH
    half = R // 2

    def packed(s, b):
        if b < SUB:
            return s * SUB + b
        return T * SUB + (s // 2) * SUB + (s % 2) * (SUB // 2) + b - SUB

    def query_slot(s, h, b):
        base = s * LH * R
        if b < SUB:
            return base + h * SUB + b
        return base + LH * SUB + (h // 2) * SUB + (h % 2) * (SUB // 2) + b - SUB

    to_seq = np.zeros((R * H, R * H))
    to_seq_wide = np.zeros((R * H, 2 * SUB * H))
    for b in range(R):
        for s in range(T):
            for h in range(LH):
                to_seq[b * H + s * LH + h, query_slot(s, h, b)] = 1
                to_seq_wide[b * H + s * LH + h, (s * LH + h) * 2 * SUB + b] = 1
    to_head = np.zeros((half * H, half * H))
    for g in range(T):
        for h in range(LH):
            for b in range(half):
                to_head[(g * LH + h) * half + b, b * H + g * LH + h] = 1
    to_value = np.zeros((LH * T * R, LH * T * R))
    for s in range(T):
        for h in range(LH):
            for b in range(R):
                src = ((b // half) * T + s) * LH * half + h * half + b % half
                to_value[h * T * R + packed(s, b), src] = 1
    spread = np.zeros((T * R, T * R))
    own_natural = np.zeros((T * 2 * SUB, T * R))
    own_packed = np.zeros((T * 2 * SUB, T * R))
    for s in range(T):
        for b in range(R):
            spread[packed(s, b), s * R + b] = 1
            own_natural[s * 2 * SUB + b, s * R + b] = 1
            own_packed[s * 2 * SUB + b, packed(s, b)] = 1
    parts = [to_seq, to_seq_wide, to_head, to_value, spread, own_natural, own_packed]
    width = max(p.shape[1] for p in parts)
    rows, places = 0, []
    for p in parts:
        places.append((rows, p.shape[0], p.shape[1]))
        rows += -(-p.shape[0] // 16) * 16
    table = np.zeros((rows, width), np.float32)
    for p, (row, n, m) in zip(parts, places):
        table[row : row + n, :m] = p
    return table, tuple(places)


def kernel(
    cfg,
    lengths,
    tokens,
    attn_gain,
    latent_gain,
    post_attn_gain,
    ffn_gain,
    post_ffn_gain,
    routes_t,
    logits_t,
    table_h,
    cache_h,
    rope_h,
    wq_h,
    wqr_h,
    wl_h,
    wkr_h,
    wku_h,
    wvu_h,
    wo_h,
    wg_h,
    wu_h,
    wd_h,
    out_result,
    out_latent,
    out_rope,
    table,
    cache,
    rope,
    wall,
    wkr,
    wku,
    wvu,
    wo,
    wgu,
    wd,
    xg,
    rows_all,
    gains,
    qsend,
    qrecv,
    qs,
    qt,
    nlat,
    nrope,
    hl,
    hsend,
    hrecv,
    asend,
    arecv,
    srecv,
    mxsend,
    mxrecv,
    sl,
    xr,
    part,
    s1,
    xsend,
    xrecv,
    rsend,
    ret,
    msend,
    mrecv,
    ku3,
    vu3,
    wide,
    sc,
    pb,
    w_sem,
    tp_send,
    tp_recv,
    d_send,
    d_recv,
    x_send,
    x_recv,
    sib_send,
    sib_recv,
    s1_send,
    s1_recv,
    rx_send,
    rx_recv,
    ret_send,
    ret_recv,
):
    T, EP, R, LH, CP, scale, places = cfg
    H = T * LH
    t = lax.axis_index("tp")
    e = lax.axis_index("ep")
    C = wku.shape[0]
    KD = wku.shape[1] // LH
    RD = wkr.shape[0]
    VD = wvu.shape[1] // LH
    D, WA = wall.shape
    F = wd.shape[0]
    LC = WA - LH * KD - LH * RD
    Q = D // T
    N = T * R
    RP = 2 * SUB
    S = EP * CP
    SPAN = cache.shape[1]
    HALF = R // 2
    HR = HALF * LH
    FOLD = D // 2
    pairs = T // 2
    sib = t + 1 - 2 * lax.rem(t, 2)

    def one_hot(i):
        row, n, m = places[i]
        return table[row : row + n, :m]

    def swap(k):
        other = e
        bit = 1
        while bit < EP:
            if k & bit:
                other = other + bit - 2 * bit * lax.rem(lax.div(e, bit), 2)
            bit *= 2
        return other

    loads = {}
    for i, (name, copies) in enumerate(
        [
            (
                "wall",
                [
                    (wq_h, wall.at[:, : LH * KD]),
                    (wqr_h, wall.at[:, LH * KD : LH * KD + LH * RD]),
                    (wl_h, wall.at[:, LH * KD + LH * RD :]),
                ],
            ),
            ("wkr", [(wkr_h, wkr)]),
            ("wku", [(wku_h, ku3)]),
            ("wvu", [(wvu_h, vu3)]),
            ("wo", [(wo_h, wo)]),
            ("wgu", [(wg_h.at[0], wgu.at[:, :F]), (wu_h.at[0], wgu.at[:, F:])]),
            ("wd", [(wd_h.at[0], wd)]),
            ("table", [(table_h, table)]),
            ("cache", [(cache_h.at[b], cache.at[b]) for b in range(R)]),
            ("rope", [(rope_h, rope)]),
        ]
    ):
        loads[name] = (i, copies)
    whole = {
        "wall": wall,
        "wkr": wkr,
        "wku": ku3,
        "wvu": vu3,
        "wo": wo,
        "wgu": wgu,
        "wd": wd,
        "table": table,
        "cache": cache,
        "rope": rope,
    }

    def fetch(name):
        i, copies = loads[name]
        for src, dst in copies:
            pltpu.make_async_copy(src, dst, w_sem.at[i]).start()

    def arrive(name):
        i, _ = loads[name]
        pltpu.make_async_copy(whole[name], whole[name], w_sem.at[i]).wait()

    for name in ("wku", "wkr", "wall", "table"):
        fetch(name)

    barrier = pltpu.get_barrier_semaphore()
    for k in range(1, T):
        pl.semaphore_signal(
            barrier, inc=1, device_id={"tp": lax.rem(t + k, T)}, device_id_type=MESH
        )
    for k in range(1, EP):
        pl.semaphore_signal(
            barrier, inc=1, device_id={"ep": swap(k)}, device_id_type=MESH
        )

    def gain(ref):
        return ref[...].astype(F32)[None, :]

    def by_head_columns(source, target):
        size = source.shape[2]
        wide[...] = source[...].astype(F32).reshape(C * LH, size)
        for h in range(LH):
            target[:, h * size : (h + 1) * size] = wide[pl.ds(h, C, stride=LH), :].astype(BF16)

    def settle_recv(ref, sem):
        remote(ref, ref, sem, sem, {"tp": sib}).wait_recv()

    def settle_send(ref, sem):
        remote(ref, ref, sem, sem, {"tp": sib}).wait_send()

    def gather_tp(phase, src, dst):
        for k in range(1, T):
            peer = lax.rem(t + k, T)
            remote(
                src, dst.at[t], tp_send.at[phase], tp_recv.at[phase], {"tp": peer}
            ).start()

    def scatter_tp(phase, src, dst):
        for k in range(1, T):
            peer = lax.rem(t + k, T)
            remote(
                src.at[peer], dst.at[t], tp_send.at[phase], tp_recv.at[phase], {"tp": peer}
            ).start()
        dst[t] = src[t]

    sent_tp = []

    def finish_tp(phase, dst):
        settle_recv(dst.at[pl.ds(0, T - 1)], tp_recv.at[phase])
        sent_tp.append((phase, dst))

    token_values = jnp.concatenate(
        [tokens[...].astype(F32), jnp.zeros((RP - R, D), F32)], axis=0
    )
    left, right = token_values[SUB:, :FOLD], token_values[SUB:, FOLD:]
    xg[t] = jnp.concatenate(
        [token_values[:SUB], join_halves(left, right)], axis=1
    ).astype(BF16)
    pl.semaphore_wait(barrier, T - 1 + EP - 1)

    gather_tp(0, xg.at[t], xg)
    fetch("cache")
    fetch("rope")
    own_normed = rms_scale(token_values, gain(attn_gain)).astype(BF16)
    for i, ref in enumerate((post_attn_gain, ffn_gain)):
        gains[i : i + 1, :] = gain(ref)
    half = RD // 2
    lane = lax.broadcasted_iota(jnp.int32, (RP, RD), 1)
    row = lax.broadcasted_iota(jnp.int32, (RP, RD), 0)
    freqs = jnp.zeros((RP, RD), F32)
    for i in range(half):
        hit = (lane == i) | (lane == i + half)
        freqs = jnp.where(hit, np.float32(theta_base ** (-i / half)), freqs)
    positions = jnp.zeros((RP, RD), jnp.int32)
    for b in range(R):
        positions = jnp.where(row == b, lengths[b], positions)
    angles = positions.astype(F32) * freqs
    cosine = jnp.cos(angles)
    sine = jnp.sin(angles)
    sine = jnp.where(lane < half, -sine, sine)
    arrive("wku")
    by_head_columns(ku3, wku)
    arrive("wkr")
    key_raw = dot_nt(own_normed, wkr[...]).astype(BF16).astype(F32)
    new_rope = turn(key_raw, cosine, sine).astype(BF16)
    nrope[...] = new_rope.astype(F32)
    out_rope[...] = new_rope[:R]
    arrive("wall")
    arrive("table")
    finish_tp(0, xg)

    blocks = [xg[s, :, :D].astype(F32) for s in range(T)]
    for p in range(pairs):
        first = xg[2 * p, :, D:].astype(F32)
        second = xg[2 * p + 1, :, D:].astype(F32)
        blocks.append(
            jnp.concatenate([join_halves(first, second), join_ends(first, second)], axis=1)
        )
    rows = jnp.concatenate(blocks, axis=0)
    rows_all[...] = rows.astype(BF16)
    row_square = jnp.sum(rows * rows, axis=1, keepdims=True)
    normed = (rows * lax.rsqrt(row_square * (1.0 / D) + eps_norm) * gain(attn_gain)).astype(BF16)
    projected = dot(normed, wall[...])
    plain = projected[:, : LH * KD].astype(BF16)
    extra = projected[:, LH * KD :]
    lifted = [
        dot_nt(plain[:, h * KD : (h + 1) * KD], wku[:, h * KD : (h + 1) * KD])
        for h in range(LH)
    ]
    base = LH * C
    fold_base = base + (LH // 2) * C
    ROT = LH * RD
    for s in range(T):
        join = join_halves if s % 2 == 0 else join_ends
        top = slice(s * SUB, (s + 1) * SUB)
        rest = slice(T * SUB + (s // 2) * SUB, T * SUB + (s // 2 + 1) * SUB)
        for h in range(LH):
            qsend[s, :, h * C : (h + 1) * C] = lifted[h][top].astype(BF16)
        for h in range(0, LH, 2):
            at = base + (h // 2) * C
            qsend[s, :, at : at + C] = join(lifted[h][rest], lifted[h + 1][rest]).astype(BF16)
        at = fold_base
        qsend[s, :, at : at + ROT + LC] = extra[top].astype(BF16)
        at += ROT + LC
        tail = extra[rest]
        qsend[s, :, at : at + ROT // 2] = join(
            tail[:, : ROT // 2], tail[:, ROT // 2 : ROT]
        ).astype(BF16)
        at += ROT // 2
        tail_latent = tail[:, ROT:]
        qsend[s, :, at : at + LC] = join(tail_latent, tail_latent).astype(BF16)
    scatter_tp(1, qsend, qrecv)
    for name in ("wvu", "wo", "wgu", "wd"):
        fetch(name)
    finish_tp(1, qrecv)

    at = fold_base
    latent_raw = jnp.concatenate(
        [
            jnp.concatenate(
                [
                    qrecv[s, :, at + ROT : at + ROT + LC],
                    qrecv[s, :, at + ROT + LC + ROT // 2 :],
                ],
                axis=0,
            )
            for s in range(T)
        ],
        axis=1,
    ).astype(F32)
    new_latent = rms_scale(latent_raw, gain(latent_gain)).astype(BF16)
    out_latent[...] = new_latent[:R]
    nlat[...] = new_latent.astype(F32)
    stacked = jnp.concatenate(
        [
            qrecv[s, :, i * C : (i + 1) * C]
            for s in range(T)
            for i in range(LH + LH // 2)
        ],
        axis=0,
    )
    qs[...] = dot(one_hot(0), stacked).astype(BF16).reshape(R, H, C)
    turned = []
    for s in range(T):
        head = qrecv[s, :, at : at + ROT].astype(F32)
        fold = qrecv[s, :, at + ROT + LC : at + ROT + LC + ROT // 2].astype(F32)
        tail = jnp.concatenate([fold, pltpu.roll(fold, SUB // 2, 0)], axis=1)
        rotary = jnp.concatenate([head, tail], axis=0)
        for h in range(LH):
            turned.append(turn(rotary[:, h * RD : (h + 1) * RD], cosine, sine).astype(BF16))
    qt[...] = dot(one_hot(1), jnp.concatenate(turned, axis=0)).astype(BF16).reshape(R, H, RD)

    arrive("cache")
    arrive("rope")
    position = lax.broadcasted_iota(jnp.int32, (H, SPAN), 1)
    for part_of in range(2):
        members = range(part_of * HALF, (part_of + 1) * HALF)
        for b in members:
            scores = (dot_nt(qs[b], cache[b]) + dot(qt[b], rope[b])) * scale
            sc[b] = jnp.where(position < lengths[b], scores, -jnp.inf)
        prob_own = {}
        for b in members:
            own = (
                jnp.sum(qs[b].astype(F32) * nlat[b : b + 1, :], axis=1, keepdims=True)
                + jnp.sum(qt[b].astype(F32) * nrope[b : b + 1, :], axis=1, keepdims=True)
            ) * scale
            masked = sc[b]
            highest = jnp.maximum(jnp.max(masked, axis=1, keepdims=True), own)
            raised = jnp.exp(masked - highest)
            raised_own = jnp.exp(own - highest)
            inverse = 1.0 / (jnp.sum(raised, axis=1, keepdims=True) + raised_own)
            pb[b] = (raised * inverse).astype(BF16)
            prob_own[b] = (raised_own * inverse).astype(BF16).astype(F32)
        for b in members:
            hl[b] = (dot(pb[b], cache[b]) + prob_own[b] * nlat[b : b + 1, :]).astype(BF16)
        attended = hl[part_of * HALF : (part_of + 1) * HALF].reshape(HALF * H, C)
        hsend[part_of] = dot(one_hot(2), attended).astype(BF16).reshape(T, HR, C)
        scatter_tp(2 + part_of, hsend.at[part_of], hrecv.at[part_of])

    arrive("wvu")
    by_head_columns(vu3, wvu)
    arrive("wo")
    slot_shift = CP.bit_length() - 1
    s_sub = lax.broadcasted_iota(jnp.int32, (S, N), 0)
    e_sub = (s_sub >> slot_shift) ^ e
    c_sub = (s_sub & (CP - 1)).astype(F32)
    gi = lax.broadcasted_iota(jnp.int32, (N, N), 0)
    gj = lax.broadcasted_iota(jnp.int32, (N, N), 1)
    upper = (gi < gj).astype(F32).astype(BF16)
    lg = logits_t[...]
    lg = jnp.exp(lg - jnp.max(lg, axis=0, keepdims=True))
    weights = lg / jnp.sum(lg, axis=0, keepdims=True)
    count = jnp.zeros((S, N), F32)
    weighted = jnp.zeros((S, N), F32)
    for k in range(routes_t.shape[0]):
        hit = routes_t[k : k + 1, :] == e_sub
        count = jnp.where(hit, 1.0, count)
        weighted = jnp.where(hit, weights[k : k + 1, :], weighted)
    rank = dot(count.astype(BF16), upper)
    taken = rank == c_sub
    weighted = jnp.where(taken, weighted, 0.0)
    weighted_hi = weighted.astype(BF16)
    weighted_lo = (weighted - weighted_hi.astype(F32)).astype(BF16)
    combine_hi = dot_nt(one_hot(5), weighted_hi).astype(BF16)
    combine_lo = dot_nt(one_hot(5), weighted_lo).astype(BF16)
    dispatch = dot_nt(jnp.where(taken, count, 0.0).astype(BF16), one_hot(4)).astype(BF16)

    finish_tp(2, hrecv.at[0])
    finish_tp(3, hrecv.at[1])
    heads = dot(one_hot(3), hrecv[...].reshape(2 * T * HR, C)).astype(BF16)
    values = jnp.concatenate(
        [
            dot(heads[h * N : (h + 1) * N], wvu[:, h * VD : (h + 1) * VD]).astype(BF16)
            for h in range(LH)
        ],
        axis=1,
    )
    for q in range(T):
        asend[q] = dot(values, wo[:, q * Q : (q + 1) * Q]).astype(BF16)
    scatter_tp(4, asend, arecv)
    finish_tp(4, arecv)
    quarter_lanes = pl.ds(pl.multiple_of(t * Q, Q), Q)
    attn = arecv[0].astype(F32)
    for s in range(1, T):
        attn = attn + arecv[s].astype(F32)
    attn = attn.astype(BF16).astype(F32)
    own_tokens = rows_all[:, quarter_lanes].astype(F32)
    scaled = attn * gains[0:1, quarter_lanes]

    def row_sum(v):
        return jnp.sum(v, axis=1, keepdims=True)

    at_lane = lax.broadcasted_iota(jnp.int32, (N, LANES), 1)
    sums = jnp.where(at_lane == 0, row_sum(attn * attn), 0.0)
    sums = jnp.where(at_lane == 1, row_sum(own_tokens * scaled), sums)
    sums = jnp.where(at_lane == 2, row_sum(scaled * scaled), sums)
    sums = jnp.concatenate([sums, jnp.zeros((LANES - N, LANES), F32)], axis=0)
    srecv[t] = sums.T[:SUB]
    gather_tp(5, srecv.at[t], srecv)
    finish_tp(5, srecv)
    totals = srecv[0]
    for s in range(1, T):
        totals = totals + srecv[s]
    totals = jnp.concatenate([totals, jnp.zeros((LANES - SUB, LANES), F32)], axis=0).T[:N]
    inverse = lax.rsqrt(totals[:, 0:1] * (1.0 / D) + eps_norm)
    mixed = (own_tokens + scaled * inverse).astype(BF16)
    square = row_square + 2.0 * inverse * totals[:, 1:2] + inverse * inverse * totals[:, 2:3]
    square = jnp.maximum(square, 0.0)
    ffn_rows = (
        mixed.astype(F32)
        * lax.rsqrt(square * (1.0 / D) + eps_norm)
        * gains[1:2, quarter_lanes]
    ).astype(BF16)
    sl[...] = dot(dispatch, ffn_rows).astype(BF16).reshape(EP, CP, Q)
    order = sorted(range(1, EP), key=lambda k: (-k.bit_length(), k))
    far = EP // 2
    chunks = [range(far, EP), range(0, far)]
    for k in order:
        remote(sl.at[k], xr.at[t, k], d_send.at[0], d_recv.at[k], {"ep": swap(k)}).start()
    xr[t, 0] = sl[0]
    mxsend[...] = dot(one_hot(6), mixed).astype(BF16).reshape(T, RP, Q)
    scatter_tp(6, mxsend, mxrecv)

    def to_peer(k, j):
        return remote(
            xr.at[t, k],
            xr.at[t, k],
            x_send.at[0],
            x_recv.at[k, j],
            {"tp": lax.rem(t + 2 * j, T)},
        )

    def to_sib(c, quarter, k):
        return remote(
            xr.at[quarter, k], xr.at[quarter, k], sib_send.at[0], sib_recv.at[c], {"tp": sib}
        )

    for c, chunk in ((1, [0]), (0, order[:far]), (1, order[far:])):
        for k in chunk:
            if k:
                settle_recv(xr.at[t, k], d_recv.at[k])
            for j in range(1, pairs):
                to_peer(k, j).start()
            to_sib(c, t, k).start()

    def relay(c):
        for k in [k for k in [0] + order if (k < far) == (c == 1)]:
            for j in range(1, pairs):
                settle_recv(xr.at[t, k], x_recv.at[k, j])
                to_sib(c, lax.rem(t + T - 2 * j, T), k).start()

    def experts(c):
        lo = chunks[c][0]
        settle_recv(xr.at[pl.ds(0, pairs), pl.ds(lo, far)], sib_recv.at[c])
        block = jnp.concatenate(
            [xr[q, lo : lo + far].reshape(far * CP, Q) for q in range(T)], axis=1
        )
        both = dot(block, wgu[...])
        gate = jnp.minimum(both[:, :F], clamp_limit)
        upward = jnp.clip(both[:, F:], -clamp_limit, clamp_limit)
        active = (upward + 1.0) * gate * (1.0 / (1.0 + jnp.exp(-sigmoid_alpha * gate)))
        active = active.astype(BF16)

        def down(quarter):
            cols = pl.ds(pl.multiple_of(quarter * Q, Q), Q)
            part[quarter, lo : lo + far] = (
                dot(active, wd[:, cols]).astype(BF16).reshape(far, CP, Q)
            )

        for j in range(pairs - 1, -1, -1):
            quarter = lax.rem(sib + 2 * j, T)
            down(quarter)
            remote(
                part.at[quarter, pl.ds(lo, far)],
                s1.at[quarter, pl.ds(lo, far)],
                s1_send.at[0],
                s1_recv.at[c, j],
                {"tp": sib},
            ).start()
        for j in range(pairs - 1, -1, -1):
            down(lax.rem(t + 2 * j, T))

    def reduce_across(c):
        lo = chunks[c][0]
        for j in range(pairs - 1, 0, -1):
            quarter = lax.rem(t + 2 * j, T)
            settle_recv(s1.at[quarter, pl.ds(lo, far)], s1_recv.at[c, j])
            for k in [k for k in order + [0] if k in chunks[c]]:
                both = part[quarter, k].astype(F32) + s1[quarter, k].astype(F32)
                xsend[j, k] = both.astype(BF16)
                remote(
                    xsend.at[j, k], xrecv.at[j, k], rx_send.at[0], rx_recv.at[k, j], {"tp": quarter}
                ).start()

    def send_back(c):
        lo = chunks[c][0]
        settle_recv(s1.at[t, pl.ds(lo, far)], s1_recv.at[c, 0])
        for k in [k for k in order + [0] if k in chunks[c]]:
            total = part[t, k].astype(F32) + s1[t, k].astype(F32)
            for j in range(1, pairs):
                settle_recv(xrecv.at[j, k], rx_recv.at[k, j])
                total = total + xrecv[j, k].astype(F32)
            if k:
                rsend[k] = total.astype(BF16)
                remote(
                    rsend.at[k], ret.at[k], ret_send.at[0], ret_recv.at[0], {"ep": swap(k)}
                ).start()
            else:
                ret[0] = total.astype(BF16)

    relay(0)
    relay(1)
    arrive("wgu")
    arrive("wd")
    experts(0)
    reduce_across(0)
    experts(1)
    reduce_across(1)
    send_back(0)
    send_back(1)
    settle_recv(ret.at[pl.ds(1, EP - 1)], ret_recv.at[0])
    returned = ret[...].reshape(S, Q)
    moe_part = dot(combine_hi, returned) + dot(combine_lo, returned)
    msend[...] = moe_part.astype(BF16).reshape(T, RP, Q)
    scatter_tp(7, msend, mrecv)
    finish_tp(6, mxrecv)
    finish_tp(7, mrecv)
    moe = jnp.concatenate([mrecv[s] for s in range(T)], axis=1).astype(F32)
    mixed_own = jnp.concatenate([mxrecv[s] for s in range(T)], axis=1).astype(F32)
    out_result[...] = (mixed_own + rms_scale(moe, gain(post_ffn_gain))).astype(BF16)[:R]

    for phase, dst in sent_tp:
        settle_send(dst.at[pl.ds(0, T - 1)], tp_send.at[phase])
    settle_send(sl.at[pl.ds(1, EP - 1)], d_send.at[0])
    if pairs > 1:
        settle_send(xr.at[pl.ds(0, pairs - 1)], x_send.at[0])
        settle_send(xsend.at[pl.ds(1, pairs - 1)], rx_send.at[0])
    settle_send(xr.at[pl.ds(0, pairs)], sib_send.at[0])
    settle_send(part.at[pl.ds(0, pairs)], s1_send.at[0])
    settle_send(rsend.at[pl.ds(1, EP - 1)], ret_send.at[0])


def hand_over(result, latent, rope, out_result, out_latent, out_rope):
    out_result[...] = result[...]
    out_latent[...] = latent[...]
    out_rope[...] = rope[...]


def body(
    tokens,
    cache_latent,
    cache_rope,
    lengths,
    attn_gain,
    latent_gain,
    post_attn_gain,
    ffn_gain,
    post_ffn_gain,
    w_query,
    w_query_rot,
    w_latent,
    w_key_rot,
    w_key_up,
    w_value_up,
    w_out,
    route_logits,
    routes,
    w_gate,
    w_up,
    w_down,
):
    R, D = tokens.shape
    T = lax.axis_size("tp")
    EP = lax.axis_size("ep")
    C, LH, KD = w_key_up.shape
    RD = w_key_rot.shape[1]
    VD = w_value_up.shape[2]
    H = T * LH
    K = routes.shape[1]
    scale = (KD + RD) ** (-0.5)
    RP = 2 * SUB
    assert R == SUB + SUB // 2 and T % 2 == 0 and LH % 2 == 0
    assert EP & (EP - 1) == 0 and T * R <= LANES
    cap = (R * T * K + EP - 1) // EP + 1
    CP = 16
    while CP < cap:
        CP *= 2
    Q = D // T
    F = w_gate.shape[2]
    LC = w_latent.shape[1]
    SPAN = cache_latent.shape[1]
    N = T * R
    table, places = layout(T, R, LH)

    vm = pl.BlockSpec(memory_space=pltpu.VMEM)
    hbm = pl.BlockSpec(memory_space=pl.ANY)
    dma = pltpu.SemaphoreType.DMA
    pairs = T // 2
    ROT = LH * RD
    QW = (LH + LH // 2) * C + ROT + LC + ROT // 2 + LC

    def v(*shape, dtype=BF16):
        return pltpu.VMEM(shape, dtype)

    cfg = (T, EP, R, LH, CP, scale, places)
    outs = pl.pallas_call(
        functools.partial(kernel, cfg),
        out_shape=(
            jax.ShapeDtypeStruct((R, D), BF16),
            jax.ShapeDtypeStruct((R, C), BF16),
            jax.ShapeDtypeStruct((R, RD), BF16),
        ),
        in_specs=[pl.BlockSpec(memory_space=pltpu.SMEM)] + [vm] * 8 + [hbm] * 13,
        out_specs=(vm, vm, vm),
        scratch_shapes=[
            v(*table.shape),
            v(R, SPAN, C),
            v(R, RD, SPAN),
            v(D, LH * KD + ROT + LC),
            v(RD, D),
            v(C, LH * KD),
            v(C, LH * VD),
            v(LH * VD, D),
            v(D, 2 * F),
            v(F, D),
            v(T, SUB, D + D // 2),
            v(N, D),
            v(SUB, D, dtype=F32),
            v(T, SUB, QW),
            v(T, SUB, QW),
            v(R, H, C),
            v(R, H, RD),
            v(RP, C, dtype=F32),
            v(RP, RD, dtype=F32),
            v(R, H, C),
            v(2, T, R // 2 * LH, C),
            v(2, T, R // 2 * LH, C),
            v(T, N, Q),
            v(T, N, Q),
            v(T, SUB, LANES, dtype=F32),
            v(T, RP, Q),
            v(T, RP, Q),
            v(EP, CP, Q),
            v(T, EP, CP, Q),
            v(T, EP, CP, Q),
            v(T, EP, CP, Q),
            v(pairs, EP, CP, Q),
            v(pairs, EP, CP, Q),
            v(EP, CP, Q),
            v(EP, CP, Q),
            v(T, RP, Q),
            v(T, RP, Q),
            v(C, LH, KD),
            v(C, LH, VD),
            v(C * LH, KD, dtype=F32),
            v(R, H, SPAN, dtype=F32),
            v(R, H, SPAN),
            dma((10,)),
            dma((8,)),
            dma((8,)),
            dma((1,)),
            dma((EP,)),
            dma((1,)),
            dma((EP, pairs)),
            dma((1,)),
            dma((2,)),
            dma((1,)),
            dma((2, pairs)),
            dma((1,)),
            dma((EP, pairs)),
            dma((1,)),
            dma((1,)),
        ],
        compiler_params=pltpu.CompilerParams(
            collective_id=0, has_side_effects=True, vmem_limit_bytes=60 * 1024 * 1024
        ),
    )(
        lengths,
        tokens,
        attn_gain,
        latent_gain,
        post_attn_gain,
        ffn_gain,
        post_ffn_gain,
        routes.T,
        route_logits.T,
        jnp.asarray(table, BF16),
        cache_latent,
        cache_rope,
        w_query,
        w_query_rot,
        w_latent,
        w_key_rot.T,
        w_key_up,
        w_value_up,
        w_out,
        w_gate,
        w_up,
        w_down,
    )
    return pl.pallas_call(
        hand_over,
        out_shape=tuple(jax.ShapeDtypeStruct(o.shape, o.dtype) for o in outs),
        in_specs=[vm] * 3,
        out_specs=(vm, vm, vm),
    )(*outs)


def solution(mesh):
    return jax.shard_map(
        body,
        mesh=mesh,
        in_specs=(
            P(("ep", "tp"), None),
            P(("ep", "tp"), None, None),
            P(("ep", "tp"), None, None),
            P(("ep", "tp")),
            P(),
            P(),
            P(),
            P(),
            P(),
            P(None, "tp"),
            P(None, "tp"),
            P(None, "tp"),
            P(),
            P(None, "tp", None),
            P(None, "tp", None),
            P("tp", None),
            P("ep", None),
            P("ep", None),
            P("ep", None, "tp"),
            P("ep", None, "tp"),
            P("ep", "tp", None),
        ),
        out_specs=(P(("ep", "tp"), None), P(("ep", "tp"), None), P(("ep", "tp"), None)),
        check_vma=False,
    )
```

time: 76.2 us -> 63.6 us (0.83)
  Pallas kernels: 75.4 us -> 62.7 us
    pallas_call x1, Pallas kernels: 73.9 us -> 61.2 us  [body(): pl.pallas_call(functools.partial(kernel, cfg), out_shape=(jax.ShapeDtypeS...]
where the time goes in v1:
time: 63.6 us; the launch traced here: 63.4 us
  Pallas kernels  62.7 us (99%)
  between operations  0.65 us (1%)
    pallas_call x1, Pallas kernels, body(): pl.pallas_call(functools.partial(kernel, cfg), out_shape=(jax.ShapeDtypeS...  61.2 us
    pallas_call x1, Pallas kernels, body(): pl.pallas_call(hand_over, out_shape=tuple((jax.ShapeDtypeStruct(o.shape,...  1.5 us

profile of v1, /device:TPU:0, one launch (start us, length us, event | category | flops | bytes accessed | tf_op | source)
XLA Modules:
  0.0 63.4 jit_solution(9867773642574150313)
XLA Ops:
  0.6 61.2 %shard_map.229 = (bf16[12,2048]{1,0:T(8,128)(2,1)}, bf16[12,512]{1,0:T(8,128)(2,1)}, bf16[12,64]{1,0:T(8,128)(2,1)}) custom-call(s32[12]{0:T(128)} %lengths.1, bf16[12,2048]{1,0:T(8,128)(2,1)} %tokens.1, bf16[2048]{0:T(1024)(128)(2,1)} %attn_gain.1, bf16[512]{0:T(512)(128)(2,1)} %latent_gain.1, bf16[2048]{0:T(1024)(128)(2,1)} %post_attn_gain.1, ...), custom_call_target="tpu_custom_call" | custom-call | tf_op jit(solution)/shard_map/pallas_call | solution.py:745
  61.9 1.5 %shard_map.230 = (bf16[12,2048]{1,0:T(8,128)(2,1)}, bf16[12,512]{1,0:T(8,128)(2,1)}, bf16[12,64]{1,0:T(8,128)(2,1)}) custom-call(bf16[12,2048]{1,0:T(8,128)(2,1)} %get-tuple-element.6.result, bf16[12,512]{1,0:T(8,128)(2,1)} %get-tuple-element.7.latent, bf16[12,64]{1,0:T(8,128)(2,1)} %get-tuple-element.8.rope), custom_call_target="tpu_custom_call" | custom-call | tf_op jit(solution)/shard_map/pallas_call | solution.py:840

commit v2 on v1

--- a/solution.py
+++ b/solution.py
@@ -61,7 +61,7 @@
     return jnp.where(half_rows(upper), pltpu.roll(upper, SUB // 2, 0), lower)
 
 
-def layout(T, R, LH):
+def layout(T, R, LH, chunks, FT, REST, QL):
     H = T * LH
     half = R // 2
 
@@ -102,7 +102,18 @@
             spread[packed(s, b), s * R + b] = 1
             own_natural[s * 2 * SUB + b, s * R + b] = 1
             own_packed[s * 2 * SUB + b, packed(s, b)] = 1
+    groups, slots = [], []
+    for lo, n in chunks:
+        for k in range(n):
+            groups += [lo + k] * (FT * SUB)
+            slots += range(FT * SUB)
+        for k in range(n if REST else 0):
+            groups += [lo + k] * SUB
+            slots += [FT * SUB] * QL + [-1] * (SUB - QL)
+    group_of = np.repeat(np.array(groups)[:, None], T * R, 1)
+    slot_of = np.repeat(np.array(slots)[:, None], T * R, 1)
     parts = [to_seq, to_seq_wide, to_head, to_value, spread, own_natural, own_packed]
+    parts += [group_of, slot_of]
     width = max(p.shape[1] for p in parts)
     rows, places = 0, []
     for p in parts:
@@ -165,6 +176,7 @@
     hrecv,
     asend,
     arecv,
+    aq,
     srecv,
     mxsend,
     mxrecv,
@@ -178,6 +190,10 @@
     ret,
     msend,
     mrecv,
+    nsend,
+    nrecv,
+    lines,
+    folded,
     ku3,
     vu3,
     wide,
@@ -186,6 +202,8 @@
     w_sem,
     tp_send,
     tp_recv,
+    p_send,
+    p_recv,
     d_send,
     d_recv,
     x_send,
@@ -198,8 +216,9 @@
     rx_recv,
     ret_send,
     ret_recv,
+    met,
 ):
-    T, EP, R, LH, CP, scale, places = cfg
+    T, EP, R, LH, FT, REST, chunks, scale, places = cfg
     H = T * LH
     t = lax.axis_index("tp")
     e = lax.axis_index("ep")
@@ -213,7 +232,8 @@
     Q = D // T
     N = T * R
     RP = 2 * SUB
-    S = EP * CP
+    QL = Q // LANES
+    W = xr.shape[3]
     SPAN = cache.shape[1]
     HALF = R // 2
     HR = HALF * LH
@@ -287,10 +307,13 @@
         pl.semaphore_signal(
             barrier, inc=1, device_id={"tp": lax.rem(t + k, T)}, device_id_type=MESH
         )
-    for k in range(1, EP):
-        pl.semaphore_signal(
-            barrier, inc=1, device_id={"ep": swap(k)}, device_id_type=MESH
-        )
+    bits = [1 << i for i in range(EP.bit_length() - 1)]
+
+    def greet(sem):
+        for k in bits:
+            pl.semaphore_signal(sem, inc=1, device_id={"ep": swap(k)}, device_id_type=MESH)
+
+    greet(barrier)
 
     def gain(ref):
         return ref[...].astype(F32)[None, :]
@@ -335,11 +358,12 @@
     xg[t] = jnp.concatenate(
         [token_values[:SUB], join_halves(left, right)], axis=1
     ).astype(BF16)
-    pl.semaphore_wait(barrier, T - 1 + EP - 1)
+    pl.semaphore_wait(barrier, T - 1 + len(bits))
 
     gather_tp(0, xg.at[t], xg)
     fetch("cache")
     fetch("rope")
+    greet(met.at[0])
     own_normed = rms_scale(token_values, gain(attn_gain)).astype(BF16)
     for i, ref in enumerate((post_attn_gain, ffn_gain)):
         gains[i : i + 1, :] = gain(ref)
@@ -411,6 +435,10 @@
     scatter_tp(1, qsend, qrecv)
     for name in ("wvu", "wo", "wgu", "wd"):
         fetch(name)
+    for i in range(1, len(bits)):
+        pl.semaphore_wait(met.at[i - 1], len(bits))
+        if i < len(bits) - 1:
+            greet(met.at[i])
     finish_tp(1, qrecv)
 
     at = fold_base
@@ -476,33 +504,39 @@
         hsend[part_of] = dot(one_hot(2), attended).astype(BF16).reshape(T, HR, C)
         scatter_tp(2 + part_of, hsend.at[part_of], hrecv.at[part_of])
 
+    lines[...] = jnp.zeros_like(lines)
+    folded[...] = jnp.zeros_like(folded)
     arrive("wvu")
     by_head_columns(vu3, wvu)
     arrive("wo")
-    slot_shift = CP.bit_length() - 1
-    s_sub = lax.broadcasted_iota(jnp.int32, (S, N), 0)
-    e_sub = (s_sub >> slot_shift) ^ e
-    c_sub = (s_sub & (CP - 1)).astype(F32)
+    group_of = one_hot(7).astype(F32).astype(jnp.int32) ^ e
+    slot_of = one_hot(8).astype(F32)
     gi = lax.broadcasted_iota(jnp.int32, (N, N), 0)
     gj = lax.broadcasted_iota(jnp.int32, (N, N), 1)
     upper = (gi < gj).astype(F32).astype(BF16)
     lg = logits_t[...]
     lg = jnp.exp(lg - jnp.max(lg, axis=0, keepdims=True))
     weights = lg / jnp.sum(lg, axis=0, keepdims=True)
-    count = jnp.zeros((S, N), F32)
-    weighted = jnp.zeros((S, N), F32)
+    count = jnp.zeros(slot_of.shape, F32)
+    weighted = jnp.zeros(slot_of.shape, F32)
     for k in range(routes_t.shape[0]):
-        hit = routes_t[k : k + 1, :] == e_sub
+        hit = routes_t[k : k + 1, :] == group_of
         count = jnp.where(hit, 1.0, count)
         weighted = jnp.where(hit, weights[k : k + 1, :], weighted)
     rank = dot(count.astype(BF16), upper)
-    taken = rank == c_sub
+    taken = rank == slot_of
     weighted = jnp.where(taken, weighted, 0.0)
     weighted_hi = weighted.astype(BF16)
     weighted_lo = (weighted - weighted_hi.astype(F32)).astype(BF16)
-    combine_hi = dot_nt(one_hot(5), weighted_hi).astype(BF16)
-    combine_lo = dot_nt(one_hot(5), weighted_lo).astype(BF16)
     dispatch = dot_nt(jnp.where(taken, count, 0.0).astype(BF16), one_hot(4)).astype(BF16)
+    spans, combines = [], []
+    for lo, n in chunks:
+        first = spans[-1][1] if spans else 0
+        spans.append((first, first + n * (FT + REST) * SUB))
+        span = slice(*spans[-1])
+        combines.append(
+            [dot_nt(one_hot(5), w[span]).astype(BF16) for w in (weighted_hi, weighted_lo)]
+        )
 
     finish_tp(2, hrecv.at[0])
     finish_tp(3, hrecv.at[1])
@@ -518,17 +552,23 @@
         asend[q] = dot(values, wo[:, q * Q : (q + 1) * Q]).astype(BF16)
     scatter_tp(4, asend, arecv)
     finish_tp(4, arecv)
-    quarter_lanes = pl.ds(pl.multiple_of(t * Q, Q), Q)
     attn = arecv[0].astype(F32)
     for s in range(1, T):
         attn = attn + arecv[s].astype(F32)
+    aq[t] = attn.astype(BF16)
     attn = attn.astype(BF16).astype(F32)
-    own_tokens = rows_all[:, quarter_lanes].astype(F32)
-    scaled = attn * gains[0:1, quarter_lanes]
+
+    def lanes_of(quarter):
+        return pl.ds(pl.multiple_of(quarter * Q, Q), Q)
 
     def row_sum(v):
         return jnp.sum(v, axis=1, keepdims=True)
 
+    def scaled_branch(attn, quarter):
+        own_tokens = rows_all[:, lanes_of(quarter)].astype(F32)
+        return own_tokens, attn * gains[0:1, lanes_of(quarter)]
+
+    own_tokens, scaled = scaled_branch(attn, t)
     at_lane = lax.broadcasted_iota(jnp.int32, (N, LANES), 1)
     sums = jnp.where(at_lane == 0, row_sum(attn * attn), 0.0)
     sums = jnp.where(at_lane == 1, row_sum(own_tokens * scaled), sums)
@@ -536,147 +576,260 @@
     sums = jnp.concatenate([sums, jnp.zeros((LANES - N, LANES), F32)], axis=0)
     srecv[t] = sums.T[:SUB]
     gather_tp(5, srecv.at[t], srecv)
+    for j in range(1, pairs):
+        remote(
+            aq.at[t], aq.at[t], p_send.at[0], p_recv.at[j], {"tp": lax.rem(t + 2 * j, T)}
+        ).start()
     finish_tp(5, srecv)
     totals = srecv[0]
     for s in range(1, T):
         totals = totals + srecv[s]
     totals = jnp.concatenate([totals, jnp.zeros((LANES - SUB, LANES), F32)], axis=0).T[:N]
     inverse = lax.rsqrt(totals[:, 0:1] * (1.0 / D) + eps_norm)
-    mixed = (own_tokens + scaled * inverse).astype(BF16)
     square = row_square + 2.0 * inverse * totals[:, 1:2] + inverse * inverse * totals[:, 2:3]
     square = jnp.maximum(square, 0.0)
-    ffn_rows = (
-        mixed.astype(F32)
-        * lax.rsqrt(square * (1.0 / D) + eps_norm)
-        * gains[1:2, quarter_lanes]
-    ).astype(BF16)
-    sl[...] = dot(dispatch, ffn_rows).astype(BF16).reshape(EP, CP, Q)
-    order = sorted(range(1, EP), key=lambda k: (-k.bit_length(), k))
+    ffn_inverse = lax.rsqrt(square * (1.0 / D) + eps_norm)
+
+    def ffn_rows(own_tokens, scaled, quarter):
+        mixed = (own_tokens + scaled * inverse).astype(BF16)
+        normed = mixed.astype(F32) * ffn_inverse * gains[1:2, lanes_of(quarter)]
+        return mixed, normed.astype(BF16)
+
+    order = sorted(range(1, EP), key=lambda k: -k)
     far = EP // 2
-    chunks = [range(far, EP), range(0, far)]
-    for k in order:
-        remote(sl.at[k], xr.at[t, k], d_send.at[0], d_recv.at[k], {"ep": swap(k)}).start()
-    xr[t, 0] = sl[0]
+    far_order, near_order = order[:far], order[far:]
+
+    def quarter_at(j):
+        return lax.rem(t + 2 * j, T)
+
+    def pack_slots(j, c, normed):
+        lo, n = chunks[c]
+        picked = dot(dispatch[slice(*spans[c])], normed)
+        for k in range(n):
+            for i in range(FT):
+                at = (k * FT + i) * SUB
+                sl[j, lo + k, :, i * Q : (i + 1) * Q] = picked[at : at + SUB].astype(BF16)
+        if REST:
+            rest = picked[n * FT * SUB :]
+            line = lax.broadcasted_iota(jnp.int32, (n * SUB, LANES), 0) & (SUB - 1)
+            fold = jnp.zeros((n * SUB, LANES), F32)
+            for i in range(QL):
+                fold = jnp.where(line == i, rest[:, i * LANES : (i + 1) * LANES], fold)
+            for k in range(n):
+                sl[j, lo + k, :, FT * Q :] = fold[k * SUB : (k + 1) * SUB].astype(BF16)
+
+    mixed, normed = ffn_rows(own_tokens, scaled, t)
+    for c in range(1, len(chunks)):
+        pack_slots(0, c, normed)
+    for k in far_order:
+        remote(sl.at[0, k], xr.at[t, k], d_send.at[0], d_recv.at[k], {"ep": swap(k)}).start()
+
+    def send_near(j):
+        for k in near_order:
+            remote(
+                sl.at[j, k], xr.at[quarter_at(j), k], d_send.at[1], d_recv.at[k], {"ep": swap(k)}
+            ).start()
+        xr[quarter_at(j), 0] = sl[j, 0]
+
+    pack_slots(0, 0, normed)
+    send_near(0)
+    for j in range(1, pairs):
+        settle_recv(aq.at[0], p_recv.at[pairs - j])
+        other = quarter_at(j)
+        _, normed = ffn_rows(*scaled_branch(aq[other].astype(F32), other), other)
+        pack_slots(j, 0, normed)
+        send_near(j)
     mxsend[...] = dot(one_hot(6), mixed).astype(BF16).reshape(T, RP, Q)
     scatter_tp(6, mxsend, mxrecv)
 
-    def to_peer(k, j):
-        return remote(
-            xr.at[t, k],
-            xr.at[t, k],
-            x_send.at[0],
-            x_recv.at[k, j],
-            {"tp": lax.rem(t + 2 * j, T)},
-        )
+    chunk_of = {lo + k: c for c, (lo, n) in enumerate(chunks) for k in range(n)}
+    far_chunks = range(1, len(chunks))
+
+    def members(c):
+        lo, n = chunks[c]
+        return [k for k in order + [0] if lo <= k < lo + n]
 
     def to_sib(c, quarter, k):
-        return remote(
+        remote(
             xr.at[quarter, k], xr.at[quarter, k], sib_send.at[0], sib_recv.at[c], {"tp": sib}
-        )
-
-    for c, chunk in ((1, [0]), (0, order[:far]), (1, order[far:])):
-        for k in chunk:
-            if k:
-                settle_recv(xr.at[t, k], d_recv.at[k])
-            for j in range(1, pairs):
-                to_peer(k, j).start()
-            to_sib(c, t, k).start()
-
-    def relay(c):
-        for k in [k for k in [0] + order if (k < far) == (c == 1)]:
+        ).start()
+
+    def relay_near(k):
+        if k:
+            settle_recv(xr.at[pl.ds(0, pairs), k], d_recv.at[k])
+        for j in range(pairs):
+            to_sib(0, quarter_at(j), k)
+
+    relay_near(0)
+    for k in far_order:
+        settle_recv(xr.at[t, k], d_recv.at[k])
+        for j in range(1, pairs):
+            remote(
+                xr.at[t, k], xr.at[t, k], x_send.at[0], x_recv.at[k, j], {"tp": quarter_at(j)}
+            ).start()
+        to_sib(chunk_of[k], t, k)
+    for k in near_order[::-1]:
+        relay_near(k)
+
+    def relay_far(c):
+        for k in members(c):
             for j in range(1, pairs):
                 settle_recv(xr.at[t, k], x_recv.at[k, j])
-                to_sib(c, lax.rem(t + T - 2 * j, T), k).start()
+                to_sib(c, lax.rem(t + T - 2 * j, T), k)
+
+    def rows_of(blocks, c):
+        return [
+            blocks(k)[:, i * Q : (i + 1) * Q]
+            for k in range(chunks[c][0], sum(chunks[c]))
+            for i in range(FT)
+        ]
+
+    def folds_of(blocks, c):
+        return [blocks(k)[:, FT * Q :] for k in range(chunks[c][0], sum(chunks[c]))]
 
     def experts(c):
-        lo = chunks[c][0]
-        settle_recv(xr.at[pl.ds(0, pairs), pl.ds(lo, far)], sib_recv.at[c])
-        block = jnp.concatenate(
-            [xr[q, lo : lo + far].reshape(far * CP, Q) for q in range(T)], axis=1
-        )
+        lo, n = chunks[c]
+        settle_recv(xr.at[pl.ds(0, pairs), pl.ds(lo, n)], sib_recv.at[c])
+        block = []
+        folds = []
+        for q in range(T):
+            block.append(jnp.concatenate(rows_of(lambda k: xr.at[q, k], c), axis=0))
+            if REST:
+                for k in range(n):
+                    fold = xr[q, lo + k, :, FT * Q :].astype(F32)
+                    lines[c, q, pl.ds(k, QL, stride=SUB), :] = fold[:QL]
+                folds += [lines[c, q, i * SUB : (i + 1) * SUB, :] for i in range(QL)]
+        block = jnp.concatenate(block, axis=1)
+        if REST:
+            block = jnp.concatenate(
+                [block, jnp.concatenate(folds, axis=1).astype(BF16)], axis=0
+            )
         both = dot(block, wgu[...])
         gate = jnp.minimum(both[:, :F], clamp_limit)
         upward = jnp.clip(both[:, F:], -clamp_limit, clamp_limit)
         active = (upward + 1.0) * gate * (1.0 / (1.0 + jnp.exp(-sigmoid_alpha * gate)))
         active = active.astype(BF16)
 
-        def down(quarter):
-            cols = pl.ds(pl.multiple_of(quarter * Q, Q), Q)
-            part[quarter, lo : lo + far] = (
-                dot(active, wd[:, cols]).astype(BF16).reshape(far, CP, Q)
-            )
+        def down(quarter, step):
+            cols = lanes_of(quarter)
+            y = dot(active, wd[:, cols])
+            for k in range(n):
+                for i in range(FT):
+                    at = (k * FT + i) * SUB
+                    part[quarter, lo + k, :, i * Q : (i + 1) * Q] = y[at : at + SUB].astype(BF16)
+            if REST:
+                for i in range(QL):
+                    folded[c, step, pl.ds(i, n, stride=SUB), :] = y[
+                        n * FT * SUB : n * FT * SUB + n, i * LANES : (i + 1) * LANES
+                    ]
+                for k in range(n):
+                    fold = folded[c, step, k * SUB : (k + 1) * SUB, :]
+                    part[quarter, lo + k, :, FT * Q :] = fold.astype(BF16)
 
         for j in range(pairs - 1, -1, -1):
             quarter = lax.rem(sib + 2 * j, T)
-            down(quarter)
+            down(quarter, j)
             remote(
-                part.at[quarter, pl.ds(lo, far)],
-                s1.at[quarter, pl.ds(lo, far)],
+                part.at[quarter, pl.ds(lo, n)],
+                s1.at[quarter, pl.ds(lo, n)],
                 s1_send.at[0],
                 s1_recv.at[c, j],
                 {"tp": sib},
             ).start()
         for j in range(pairs - 1, -1, -1):
-            down(lax.rem(t + 2 * j, T))
-
-    def reduce_across(c):
-        lo = chunks[c][0]
+            down(quarter_at(j), pairs + j)
+
+    def chip_sum(quarter, k):
+        return part[quarter, k].astype(F32) + s1[quarter, k].astype(F32)
+
+    def return_near():
+        for j in range(pairs):
+            settle_recv(s1.at[quarter_at(j), pl.ds(0, far)], s1_recv.at[0, j])
+        for k in near_order:
+            for j in range(pairs):
+                rsend[j, k] = chip_sum(quarter_at(j), k).astype(BF16)
+                remote(
+                    rsend.at[j, k], ret.at[j, k], ret_send.at[1], ret_recv.at[1], {"ep": swap(k)}
+                ).start()
+        for j in range(pairs):
+            ret[j, 0] = chip_sum(quarter_at(j), 0).astype(BF16)
+
+    def reduce_far(c):
+        lo, n = chunks[c]
         for j in range(pairs - 1, 0, -1):
-            quarter = lax.rem(t + 2 * j, T)
-            settle_recv(s1.at[quarter, pl.ds(lo, far)], s1_recv.at[c, j])
-            for k in [k for k in order + [0] if k in chunks[c]]:
-                both = part[quarter, k].astype(F32) + s1[quarter, k].astype(F32)
-                xsend[j, k] = both.astype(BF16)
+            quarter = quarter_at(j)
+            settle_recv(s1.at[quarter, pl.ds(lo, n)], s1_recv.at[c, j])
+            for k in members(c):
+                xsend[j, k] = chip_sum(quarter, k).astype(BF16)
                 remote(
                     xsend.at[j, k], xrecv.at[j, k], rx_send.at[0], rx_recv.at[k, j], {"tp": quarter}
                 ).start()
 
-    def send_back(c):
-        lo = chunks[c][0]
-        settle_recv(s1.at[t, pl.ds(lo, far)], s1_recv.at[c, 0])
-        for k in [k for k in order + [0] if k in chunks[c]]:
-            total = part[t, k].astype(F32) + s1[t, k].astype(F32)
+    def return_far(c):
+        lo, n = chunks[c]
+        settle_recv(s1.at[t, pl.ds(lo, n)], s1_recv.at[c, 0])
+        for k in members(c):
+            total = chip_sum(t, k)
             for j in range(1, pairs):
                 settle_recv(xrecv.at[j, k], rx_recv.at[k, j])
                 total = total + xrecv[j, k].astype(F32)
-            if k:
-                rsend[k] = total.astype(BF16)
-                remote(
-                    rsend.at[k], ret.at[k], ret_send.at[0], ret_recv.at[0], {"ep": swap(k)}
-                ).start()
-            else:
-                ret[0] = total.astype(BF16)
-
-    relay(0)
-    relay(1)
+            rsend[0, k] = total.astype(BF16)
+            remote(
+                rsend.at[0, k], ret.at[0, k], ret_send.at[0], ret_recv.at[0], {"ep": swap(k)}
+            ).start()
+
+    def combine(j, c):
+        rows = rows_of(lambda k: ret.at[j, k], c)
+        if REST:
+            n = chunks[c][1]
+            fold = jnp.concatenate(folds_of(lambda k: ret.at[j, k], c), axis=0).astype(F32)
+            line = lax.broadcasted_iota(jnp.int32, (n * SUB, LANES), 0) & (SUB - 1)
+            lanes = [jnp.where(line == i, fold, 0.0).astype(BF16) for i in range(QL)]
+            rows.append(jnp.concatenate(lanes, axis=1))
+        rows = jnp.concatenate(rows, axis=0)
+        return sum(dot(w, rows) for w in combines[c])
+
     arrive("wgu")
     arrive("wd")
     experts(0)
-    reduce_across(0)
+    relay_far(1)
+    return_near()
     experts(1)
-    reduce_across(1)
-    send_back(0)
-    send_back(1)
-    settle_recv(ret.at[pl.ds(1, EP - 1)], ret_recv.at[0])
-    returned = ret[...].reshape(S, Q)
-    moe_part = dot(combine_hi, returned) + dot(combine_lo, returned)
-    msend[...] = moe_part.astype(BF16).reshape(T, RP, Q)
+    reduce_far(1)
+    return_far(1)
+    settle_recv(ret.at[pl.ds(0, pairs), pl.ds(1, far - 1)], ret_recv.at[1])
+    for j in range(pairs):
+        nsend[:, j] = combine(j, 0).astype(BF16).reshape(T, RP, Q)
+    scatter_tp(8, nsend, nrecv)
+    settle_recv(ret.at[0, pl.ds(far, far)], ret_recv.at[0])
+    far_part = sum(combine(0, c) for c in far_chunks)
+    msend[...] = far_part.astype(BF16).reshape(T, RP, Q)
     scatter_tp(7, msend, mrecv)
     finish_tp(6, mxrecv)
+    finish_tp(8, nrecv)
     finish_tp(7, mrecv)
-    moe = jnp.concatenate([mrecv[s] for s in range(T)], axis=1).astype(F32)
+    moe = []
+    for q in range(T):
+        total = mrecv[q].astype(F32)
+        for j in range(pairs):
+            total = total + nrecv[(q + T - 2 * j) % T, j].astype(F32)
+        moe.append(total)
+    moe = jnp.concatenate(moe, axis=1).astype(BF16).astype(F32)
     mixed_own = jnp.concatenate([mxrecv[s] for s in range(T)], axis=1).astype(F32)
     out_result[...] = (mixed_own + rms_scale(moe, gain(post_ffn_gain))).astype(BF16)[:R]
 
     for phase, dst in sent_tp:
         settle_send(dst.at[pl.ds(0, T - 1)], tp_send.at[phase])
-    settle_send(sl.at[pl.ds(1, EP - 1)], d_send.at[0])
+    settle_send(xr.at[0, pl.ds(0, far)], d_send.at[0])
+    settle_send(xr.at[pl.ds(0, pairs), pl.ds(1, far - 1)], d_send.at[1])
     if pairs > 1:
-        settle_send(xr.at[pl.ds(0, pairs - 1)], x_send.at[0])
-        settle_send(xsend.at[pl.ds(1, pairs - 1)], rx_send.at[0])
+        settle_send(aq.at[pl.ds(0, pairs - 1)], p_send.at[0])
+        settle_send(xr.at[pl.ds(0, pairs - 1), pl.ds(0, far)], x_send.at[0])
+        settle_send(xsend.at[pl.ds(1, pairs - 1), pl.ds(0, far)], rx_send.at[0])
     settle_send(xr.at[pl.ds(0, pairs)], sib_send.at[0])
     settle_send(part.at[pl.ds(0, pairs)], s1_send.at[0])
-    settle_send(rsend.at[pl.ds(1, EP - 1)], ret_send.at[0])
+    settle_send(xr.at[0, pl.ds(0, far)], ret_send.at[0])
+    settle_send(xr.at[pl.ds(0, pairs), pl.ds(1, far - 1)], ret_send.at[1])
 
 
 def hand_over(result, latent, rope, out_result, out_latent, out_rope):
@@ -721,15 +874,19 @@
     assert R == SUB + SUB // 2 and T % 2 == 0 and LH % 2 == 0
     assert EP & (EP - 1) == 0 and T * R <= LANES
     cap = (R * T * K + EP - 1) // EP + 1
-    CP = 16
-    while CP < cap:
-        CP *= 2
     Q = D // T
     F = w_gate.shape[2]
     LC = w_latent.shape[1]
     SPAN = cache_latent.shape[1]
     N = T * R
-    table, places = layout(T, R, LH)
+    QL = Q // LANES
+    FT, REST = cap // SUB, cap % SUB
+    if REST > 1 or QL > SUB:
+        FT, REST = -(-cap // SUB), 0
+    W = FT * Q + REST * LANES
+    far = EP // 2
+    chunks = ((0, far), (far, far))
+    table, places = layout(T, R, LH, chunks, FT, REST, QL)
 
     vm = pl.BlockSpec(memory_space=pltpu.VMEM)
     hbm = pl.BlockSpec(memory_space=pl.ANY)
@@ -741,7 +898,7 @@
     def v(*shape, dtype=BF16):
         return pltpu.VMEM(shape, dtype)
 
-    cfg = (T, EP, R, LH, CP, scale, places)
+    cfg = (T, EP, R, LH, FT, REST, chunks, scale, places)
     outs = pl.pallas_call(
         functools.partial(kernel, cfg),
         out_shape=(
@@ -776,39 +933,47 @@
             v(2, T, R // 2 * LH, C),
             v(T, N, Q),
             v(T, N, Q),
+            v(T, N, Q),
             v(T, SUB, LANES, dtype=F32),
             v(T, RP, Q),
             v(T, RP, Q),
-            v(EP, CP, Q),
-            v(T, EP, CP, Q),
-            v(T, EP, CP, Q),
-            v(T, EP, CP, Q),
-            v(pairs, EP, CP, Q),
-            v(pairs, EP, CP, Q),
-            v(EP, CP, Q),
-            v(EP, CP, Q),
+            v(pairs, EP, SUB, W),
+            v(T, EP, SUB, W),
+            v(T, EP, SUB, W),
+            v(T, EP, SUB, W),
+            v(pairs, EP, SUB, W),
+            v(pairs, EP, SUB, W),
+            v(pairs, EP, SUB, W),
+            v(pairs, EP, SUB, W),
             v(T, RP, Q),
             v(T, RP, Q),
+            v(T, pairs, RP, Q),
+            v(T, pairs, RP, Q),
+            v(len(chunks), T, QL * SUB, LANES, dtype=F32),
+            v(len(chunks), T, far * SUB, LANES, dtype=F32),
             v(C, LH, KD),
             v(C, LH, VD),
             v(C * LH, KD, dtype=F32),
             v(R, H, SPAN, dtype=F32),
             v(R, H, SPAN),
             dma((10,)),
-            dma((8,)),
-            dma((8,)),
+            dma((9,)),
+            dma((9,)),
             dma((1,)),
+            dma((pairs,)),
+            dma((2,)),
             dma((EP,)),
             dma((1,)),
             dma((EP, pairs)),
             dma((1,)),
-            dma((2,)),
+            dma((len(chunks),)),
             dma((1,)),
-            dma((2, pairs)),
+            dma((len(chunks), pairs)),
             dma((1,)),
             dma((EP, pairs)),
-            dma((1,)),
-            dma((1,)),
+            dma((2,)),
+            dma((2,)),
+            pltpu.SemaphoreType.REGULAR((max(1, EP.bit_length() - 2),)),
         ],
         compiler_params=pltpu.CompilerParams(
             collective_id=0, has_side_effects=True, vmem_limit_bytes=60 * 1024 * 1024

time: 63.6 us -> 60.2 us (0.947)
  Pallas kernels: 62.7 us -> 59.3 us
    pallas_call x1, Pallas kernels: 61.2 us -> 57.8 us  [body(): pl.pallas_call(functools.partial(kernel, cfg), out_shape=(jax.ShapeDtypeS...]
where the time goes in v2:
time: 60.2 us; the launch traced here: 60 us
  Pallas kernels  59.3 us (99%)
  between operations  0.65 us (1%)
    pallas_call x1, Pallas kernels, body(): pl.pallas_call(functools.partial(kernel, cfg), out_shape=(jax.ShapeDtypeS...  57.8 us
    pallas_call x1, Pallas kernels, body(): pl.pallas_call(hand_over, out_shape=tuple((jax.ShapeDtypeStruct(o.shape,...  1.5 us

profile of v2, /device:TPU:0, one launch (start us, length us, event | category | flops | bytes accessed | tf_op | source)
XLA Modules:
  0.0 60.0 jit_solution(11408494556828866902)
XLA Ops:
  0.6 57.8 %shard_map.229 = (bf16[12,2048]{1,0:T(8,128)(2,1)}, bf16[12,512]{1,0:T(8,128)(2,1)}, bf16[12,64]{1,0:T(8,128)(2,1)}) custom-call(s32[12]{0:T(128)} %lengths.1, bf16[12,2048]{1,0:T(8,128)(2,1)} %tokens.1, bf16[2048]{0:T(1024)(128)(2,1)} %attn_gain.1, bf16[512]{0:T(512)(128)(2,1)} %latent_gain.1, bf16[2048]{0:T(1024)(128)(2,1)} %post_attn_gain.1, ...), custom_call_target="tpu_custom_call" | custom-call | tf_op jit(solution)/shard_map/pallas_call | solution.py:902
  58.5 1.5 %shard_map.230 = (bf16[12,2048]{1,0:T(8,128)(2,1)}, bf16[12,512]{1,0:T(8,128)(2,1)}, bf16[12,64]{1,0:T(8,128)(2,1)}) custom-call(bf16[12,2048]{1,0:T(8,128)(2,1)} %get-tuple-element.6.result, bf16[12,512]{1,0:T(8,128)(2,1)} %get-tuple-element.7.latent, bf16[12,64]{1,0:T(8,128)(2,1)} %get-tuple-element.8.rope), custom_call_target="tpu_custom_call" | custom-call | tf_op jit(solution)/shard_map/pallas_call | solution.py:1005

commit v3 on v2

--- a/solution.py
+++ b/solution.py
@@ -63,37 +63,35 @@
 
 def layout(T, R, LH, chunks, FT, REST, QL):
     H = T * LH
-    half = R // 2
+    tail = R - SUB
+    mid = LH // 2
 
     def packed(s, b):
         if b < SUB:
             return s * SUB + b
-        return T * SUB + (s // 2) * SUB + (s % 2) * (SUB // 2) + b - SUB
-
-    def query_slot(s, h, b):
-        base = s * LH * R
-        if b < SUB:
-            return base + h * SUB + b
-        return base + LH * SUB + (h // 2) * SUB + (h % 2) * (SUB // 2) + b - SUB
-
-    to_seq = np.zeros((R * H, R * H))
-    to_seq_wide = np.zeros((R * H, 2 * SUB * H))
-    for b in range(R):
-        for s in range(T):
-            for h in range(LH):
-                to_seq[b * H + s * LH + h, query_slot(s, h, b)] = 1
-                to_seq_wide[b * H + s * LH + h, (s * LH + h) * 2 * SUB + b] = 1
-    to_head = np.zeros((half * H, half * H))
-    for g in range(T):
-        for h in range(LH):
-            for b in range(half):
-                to_head[(g * LH + h) * half + b, b * H + g * LH + h] = 1
+        return T * SUB + (s // 2) * SUB + (s % 2) * tail + b - SUB
+
+    to_seq = np.zeros((SUB * H, H * SUB))
+    to_seq_tail = np.zeros((tail * H, T * mid * SUB))
+    to_turn_tail = np.zeros((tail * H, T * mid * SUB))
+    to_head = np.zeros((H * SUB, SUB * H))
+    to_head_tail = np.zeros((H * tail, tail * H))
     to_value = np.zeros((LH * T * R, LH * T * R))
     for s in range(T):
         for h in range(LH):
-            for b in range(R):
-                src = ((b // half) * T + s) * LH * half + h * half + b % half
-                to_value[h * T * R + packed(s, b), src] = 1
+            head = s * LH + h
+            for b in range(SUB):
+                to_seq[b * H + head, head * SUB + b] = 1
+                to_head[head * SUB + b, b * H + head] = 1
+                to_value[h * T * R + packed(s, b), head * SUB + b] = 1
+            for b in range(tail):
+                at = (s * mid + h // 2) * SUB + (h % 2) * tail + b
+                to_seq_tail[b * H + head, at] = 1
+                at = (s * mid + h % mid) * SUB + (h // mid) * tail + b
+                to_turn_tail[b * H + head, at] = 1
+                to_head_tail[head * tail + b, b * H + head] = 1
+                at = H * SUB + head * tail + b
+                to_value[h * T * R + packed(s, SUB + b), at] = 1
     spread = np.zeros((T * R, T * R))
     own_natural = np.zeros((T * 2 * SUB, T * R))
     own_packed = np.zeros((T * 2 * SUB, T * R))
@@ -112,8 +110,8 @@
             slots += [FT * SUB] * QL + [-1] * (SUB - QL)
     group_of = np.repeat(np.array(groups)[:, None], T * R, 1)
     slot_of = np.repeat(np.array(slots)[:, None], T * R, 1)
-    parts = [to_seq, to_seq_wide, to_head, to_value, spread, own_natural, own_packed]
-    parts += [group_of, slot_of]
+    parts = [to_seq, to_seq_tail, to_turn_tail, to_value, spread, own_natural, own_packed]
+    parts += [group_of, slot_of, to_head, to_head_tail]
     width = max(p.shape[1] for p in parts)
     rows, places = 0, []
     for p in parts:
@@ -127,15 +125,15 @@
 
 def kernel(
     cfg,
-    lengths,
-    tokens,
-    attn_gain,
-    latent_gain,
-    post_attn_gain,
-    ffn_gain,
-    post_ffn_gain,
-    routes_t,
-    logits_t,
+    lengths_h,
+    tokens_h,
+    attn_gain_h,
+    latent_gain_h,
+    post_attn_gain_h,
+    ffn_gain_h,
+    post_ffn_gain_h,
+    routes_t_h,
+    logits_t_h,
     table_h,
     cache_h,
     rope_h,
@@ -149,6 +147,18 @@
     wg_h,
     wu_h,
     wd_h,
+    out_result_h,
+    out_latent_h,
+    out_rope_h,
+    lengths,
+    tokens,
+    attn_gain,
+    latent_gain,
+    post_attn_gain,
+    ffn_gain,
+    post_ffn_gain,
+    routes_t,
+    logits_t,
     out_result,
     out_latent,
     out_rope,
@@ -174,6 +184,8 @@
     hl,
     hsend,
     hrecv,
+    hsend_tail,
+    hrecv_tail,
     asend,
     arecv,
     aq,
@@ -235,8 +247,8 @@
     QL = Q // LANES
     W = xr.shape[3]
     SPAN = cache.shape[1]
-    HALF = R // 2
-    HR = HALF * LH
+    tail = R - SUB
+    mid = LH // 2
     FOLD = D // 2
     pairs = T // 2
     sib = t + 1 - 2 * lax.rem(t, 2)
@@ -274,21 +286,26 @@
             ("table", [(table_h, table)]),
             ("cache", [(cache_h.at[b], cache.at[b]) for b in range(R)]),
             ("rope", [(rope_h, rope)]),
+            ("tokens", [(tokens_h, tokens)]),
+            ("lengths", [(lengths_h, lengths)]),
+            ("attn_gain", [(attn_gain_h, attn_gain)]),
+            ("latent_gain", [(latent_gain_h, latent_gain)]),
+            ("post_attn_gain", [(post_attn_gain_h, post_attn_gain)]),
+            ("ffn_gain", [(ffn_gain_h, ffn_gain)]),
+            ("post_ffn_gain", [(post_ffn_gain_h, post_ffn_gain)]),
+            ("routes", [(routes_t_h, routes_t)]),
+            ("logits", [(logits_t_h, logits_t)]),
         ]
     ):
         loads[name] = (i, copies)
-    whole = {
-        "wall": wall,
-        "wkr": wkr,
-        "wku": ku3,
-        "wvu": vu3,
-        "wo": wo,
-        "wgu": wgu,
-        "wd": wd,
-        "table": table,
-        "cache": cache,
-        "rope": rope,
-    }
+    for name, copies in (
+        ("out_rope", (out_rope, out_rope_h)),
+        ("out_latent", (out_latent, out_latent_h)),
+        ("out_result", (out_result, out_result_h)),
+    ):
+        earlier = {"out_rope": "tokens", "out_latent": "wall", "out_result": "wkr"}[name]
+        loads[name] = (loads[earlier][0], [copies])
+    whole = {"wall": wall, "wgu": wgu, "cache": cache}
 
     def fetch(name):
         i, copies = loads[name]
@@ -296,12 +313,11 @@
             pltpu.make_async_copy(src, dst, w_sem.at[i]).start()
 
     def arrive(name):
-        i, _ = loads[name]
-        pltpu.make_async_copy(whole[name], whole[name], w_sem.at[i]).wait()
-
-    for name in ("wku", "wkr", "wall", "table"):
-        fetch(name)
-
+        i, copies = loads[name]
+        src, dst = (whole[name], whole[name]) if name in whole else copies[0]
+        pltpu.make_async_copy(src, dst, w_sem.at[i]).wait()
+
+    fetch("tokens")
     barrier = pltpu.get_barrier_semaphore()
     for k in range(1, T):
         pl.semaphore_signal(
@@ -314,6 +330,10 @@
             pl.semaphore_signal(sem, inc=1, device_id={"ep": swap(k)}, device_id_type=MESH)
 
     greet(barrier)
+    for name in ("attn_gain", "lengths", "post_attn_gain", "ffn_gain", "latent_gain"):
+        fetch(name)
+    for name in ("wku", "wkr", "wall", "table", "post_ffn_gain", "routes", "logits"):
+        fetch(name)
 
     def gain(ref):
         return ref[...].astype(F32)[None, :]
@@ -330,27 +350,39 @@
     def settle_send(ref, sem):
         remote(ref, ref, sem, sem, {"tp": sib}).wait_send()
 
+    sent_tp = {}
+    send_of = {0: 0, 1: 1, 9: 2, 2: 0, 3: 1, 4: 2, 5: 0, 6: 1, 8: 2, 7: 0}
+
+    def reuse_send(phase):
+        slot = send_of[phase]
+        if slot in sent_tp:
+            settle_send(sent_tp.pop(slot), tp_send.at[slot])
+        return tp_send.at[slot]
+
+    peers = [lax.rem(c + 2 * j, T) for c in (t, sib) for j in range(1, pairs)] + [sib]
+
     def gather_tp(phase, src, dst):
-        for k in range(1, T):
-            peer = lax.rem(t + k, T)
+        sent = reuse_send(phase)
+        for peer in peers:
             remote(
-                src, dst.at[t], tp_send.at[phase], tp_recv.at[phase], {"tp": peer}
+                src, dst.at[t], sent, tp_recv.at[phase], {"tp": peer}
             ).start()
 
     def scatter_tp(phase, src, dst):
-        for k in range(1, T):
-            peer = lax.rem(t + k, T)
+        sent = reuse_send(phase)
+        for peer in peers:
             remote(
-                src.at[peer], dst.at[t], tp_send.at[phase], tp_recv.at[phase], {"tp": peer}
+                src.at[peer], dst.at[t], sent, tp_recv.at[phase], {"tp": peer}
             ).start()
         dst[t] = src[t]
 
-    sent_tp = []
-
-    def finish_tp(phase, dst):
-        settle_recv(dst.at[pl.ds(0, T - 1)], tp_recv.at[phase])
-        sent_tp.append((phase, dst))
-
+
+    def finish_tp(phase, dst, lanes=None):
+        view = dst.at[pl.ds(0, T - 1)] if lanes is None else dst.at[pl.ds(0, T - 1), :, lanes]
+        settle_recv(view, tp_recv.at[phase])
+        sent_tp[send_of[phase]] = view
+
+    arrive("tokens")
     token_values = jnp.concatenate(
         [tokens[...].astype(F32), jnp.zeros((RP - R, D), F32)], axis=0
     )
@@ -364,6 +396,8 @@
     fetch("cache")
     fetch("rope")
     greet(met.at[0])
+    for name in ("attn_gain", "lengths", "post_attn_gain", "ffn_gain"):
+        arrive(name)
     own_normed = rms_scale(token_values, gain(attn_gain)).astype(BF16)
     for i, ref in enumerate((post_attn_gain, ffn_gain)):
         gains[i : i + 1, :] = gain(ref)
@@ -388,6 +422,7 @@
     new_rope = turn(key_raw, cosine, sine).astype(BF16)
     nrope[...] = new_rope.astype(F32)
     out_rope[...] = new_rope[:R]
+    fetch("out_rope")
     arrive("wall")
     arrive("table")
     finish_tp(0, xg)
@@ -410,78 +445,99 @@
         dot_nt(plain[:, h * KD : (h + 1) * KD], wku[:, h * KD : (h + 1) * KD])
         for h in range(LH)
     ]
-    base = LH * C
-    fold_base = base + (LH // 2) * C
     ROT = LH * RD
+    split = LH * C + ROT + LC
+    turn_tail = split + mid * C
+    early, late = pl.ds(0, split), pl.ds(split, qsend.shape[2] - split)
+
+    def send_queries(phase, lanes):
+        sent = reuse_send(phase)
+        for peer in peers:
+            remote(
+                qsend.at[peer, :, lanes],
+                qrecv.at[t, :, lanes],
+                sent,
+                tp_recv.at[phase],
+                {"tp": peer},
+            ).start()
+
+    for s in range(T):
+        top = slice(s * SUB, (s + 1) * SUB)
+        for h in range(LH):
+            qsend[s, :, h * C : (h + 1) * C] = lifted[h][top].astype(BF16)
+        qsend[s, :, LH * C : split] = extra[top].astype(BF16)
+    send_queries(1, early)
     for s in range(T):
         join = join_halves if s % 2 == 0 else join_ends
-        top = slice(s * SUB, (s + 1) * SUB)
         rest = slice(T * SUB + (s // 2) * SUB, T * SUB + (s // 2 + 1) * SUB)
-        for h in range(LH):
-            qsend[s, :, h * C : (h + 1) * C] = lifted[h][top].astype(BF16)
         for h in range(0, LH, 2):
-            at = base + (h // 2) * C
+            at = split + (h // 2) * C
             qsend[s, :, at : at + C] = join(lifted[h][rest], lifted[h + 1][rest]).astype(BF16)
-        at = fold_base
-        qsend[s, :, at : at + ROT + LC] = extra[top].astype(BF16)
-        at += ROT + LC
-        tail = extra[rest]
+        last = extra[rest]
+        at = turn_tail
         qsend[s, :, at : at + ROT // 2] = join(
-            tail[:, : ROT // 2], tail[:, ROT // 2 : ROT]
+            last[:, : ROT // 2], last[:, ROT // 2 : ROT]
         ).astype(BF16)
         at += ROT // 2
-        tail_latent = tail[:, ROT:]
-        qsend[s, :, at : at + LC] = join(tail_latent, tail_latent).astype(BF16)
-    scatter_tp(1, qsend, qrecv)
+        last = last[:, ROT:]
+        qsend[s, :, at : at + LC] = join(last, last).astype(BF16)
+    send_queries(9, late)
+    qrecv[t] = qsend[t]
     for name in ("wvu", "wo", "wgu", "wd"):
         fetch(name)
     for i in range(1, len(bits)):
         pl.semaphore_wait(met.at[i - 1], len(bits))
         if i < len(bits) - 1:
             greet(met.at[i])
-    finish_tp(1, qrecv)
-
-    at = fold_base
-    latent_raw = jnp.concatenate(
-        [
-            jnp.concatenate(
-                [
-                    qrecv[s, :, at + ROT : at + ROT + LC],
-                    qrecv[s, :, at + ROT + LC + ROT // 2 :],
-                ],
-                axis=0,
-            )
+    finish_tp(1, qrecv, early)
+
+    arrive("latent_gain")
+
+    def fresh_latent(at):
+        raw = jnp.concatenate([qrecv[s, :, at : at + LC] for s in range(T)], axis=1)
+        return rms_scale(raw.astype(F32), gain(latent_gain)).astype(BF16)
+
+    def queries(first, table_of, blocks):
+        stacked = jnp.concatenate(blocks, axis=0)
+        rows = dot(table_of, stacked).astype(BF16)
+        return rows.reshape(first, H, stacked.shape[1])
+
+    def turned(at, count, cosine, sine):
+        return [
+            turn(qrecv[s, :, at + i * RD : at + (i + 1) * RD].astype(F32), cosine, sine).astype(BF16)
             for s in range(T)
-        ],
-        axis=1,
-    ).astype(F32)
-    new_latent = rms_scale(latent_raw, gain(latent_gain)).astype(BF16)
-    out_latent[...] = new_latent[:R]
-    nlat[...] = new_latent.astype(F32)
-    stacked = jnp.concatenate(
-        [
-            qrecv[s, :, i * C : (i + 1) * C]
-            for s in range(T)
-            for i in range(LH + LH // 2)
-        ],
-        axis=0,
-    )
-    qs[...] = dot(one_hot(0), stacked).astype(BF16).reshape(R, H, C)
-    turned = []
-    for s in range(T):
-        head = qrecv[s, :, at : at + ROT].astype(F32)
-        fold = qrecv[s, :, at + ROT + LC : at + ROT + LC + ROT // 2].astype(F32)
-        tail = jnp.concatenate([fold, pltpu.roll(fold, SUB // 2, 0)], axis=1)
-        rotary = jnp.concatenate([head, tail], axis=0)
-        for h in range(LH):
-            turned.append(turn(rotary[:, h * RD : (h + 1) * RD], cosine, sine).astype(BF16))
-    qt[...] = dot(one_hot(1), jnp.concatenate(turned, axis=0)).astype(BF16).reshape(R, H, RD)
+            for i in range(count)
+        ]
+
+    def blocks_of(at, count):
+        return [qrecv[s, :, at + i * C : at + (i + 1) * C] for s in range(T) for i in range(count)]
+
+    latent = fresh_latent(LH * C + ROT)
+    out_latent[:SUB] = latent
+    nlat[:SUB] = latent.astype(F32)
+    qs[:SUB] = queries(SUB, one_hot(0), blocks_of(0, LH))
+    qt[:SUB] = queries(SUB, one_hot(0), turned(LH * C, LH, cosine[:SUB], sine[:SUB]))
+
+    def late_queries():
+        finish_tp(9, qrecv, late)
+        latent = fresh_latent(turn_tail + ROT // 2)
+        out_latent[SUB:] = latent[:tail]
+        fetch("out_latent")
+        nlat[SUB:] = latent.astype(F32)
+        qs[SUB:] = queries(tail, one_hot(1), blocks_of(split, mid))
+        cos, sin = cosine[SUB:], sine[SUB:]
+        cos, sin = join_halves(cos, cos), join_halves(sin, sin)
+        qt[SUB:] = queries(tail, one_hot(2), turned(turn_tail, mid, cos, sin))
 
     arrive("cache")
     arrive("rope")
     position = lax.broadcasted_iota(jnp.int32, (H, SPAN), 1)
-    for part_of in range(2):
-        members = range(part_of * HALF, (part_of + 1) * HALF)
+    for members, table_of, phase, send, recv in (
+        (range(SUB), one_hot(9), 2, hsend, hrecv),
+        (range(SUB, R), one_hot(10), 3, hsend_tail, hrecv_tail),
+    ):
+        if phase == 3:
+            late_queries()
         for b in members:
             scores = (dot_nt(qs[b], cache[b]) + dot(qt[b], rope[b])) * scale
             sc[b] = jnp.where(position < lengths[b], scores, -jnp.inf)
@@ -500,13 +556,15 @@
             prob_own[b] = (raised_own * inverse).astype(BF16).astype(F32)
         for b in members:
             hl[b] = (dot(pb[b], cache[b]) + prob_own[b] * nlat[b : b + 1, :]).astype(BF16)
-        attended = hl[part_of * HALF : (part_of + 1) * HALF].reshape(HALF * H, C)
-        hsend[part_of] = dot(one_hot(2), attended).astype(BF16).reshape(T, HR, C)
-        scatter_tp(2 + part_of, hsend.at[part_of], hrecv.at[part_of])
+        count = len(members)
+        attended = hl[members[0] : members[0] + count].reshape(count * H, C)
+        send[...] = dot(table_of, attended).astype(BF16).reshape(T, count * LH, C)
+        scatter_tp(phase, send, recv)
 
     lines[...] = jnp.zeros_like(lines)
     folded[...] = jnp.zeros_like(folded)
-    arrive("wvu")
+    for name in ("routes", "logits", "post_ffn_gain", "wvu"):
+        arrive(name)
     by_head_columns(vu3, wvu)
     arrive("wo")
     group_of = one_hot(7).astype(F32).astype(jnp.int32) ^ e
@@ -538,9 +596,12 @@
             [dot_nt(one_hot(5), w[span]).astype(BF16) for w in (weighted_hi, weighted_lo)]
         )
 
-    finish_tp(2, hrecv.at[0])
-    finish_tp(3, hrecv.at[1])
-    heads = dot(one_hot(3), hrecv[...].reshape(2 * T * HR, C)).astype(BF16)
+    finish_tp(2, hrecv)
+    finish_tp(3, hrecv_tail)
+    attended = jnp.concatenate(
+        [hrecv[...].reshape(H * SUB, C), hrecv_tail[...].reshape(H * tail, C)], axis=0
+    )
+    heads = dot(one_hot(3), attended).astype(BF16)
     values = jnp.concatenate(
         [
             dot(heads[h * N : (h + 1) * N], wvu[:, h * VD : (h + 1) * VD]).astype(BF16)
@@ -548,18 +609,23 @@
         ],
         axis=1,
     )
-    for q in range(T):
-        asend[q] = dot(values, wo[:, q * Q : (q + 1) * Q]).astype(BF16)
-    scatter_tp(4, asend, arecv)
+
+    def lanes_of(quarter):
+        return pl.ds(pl.multiple_of(quarter * Q, Q), Q)
+
+    sent = reuse_send(4)
+    for peer in peers:
+        asend[peer] = dot(values, wo[:, lanes_of(peer)]).astype(BF16)
+        remote(
+            asend.at[peer], arecv.at[t], sent, tp_recv.at[4], {"tp": peer}
+        ).start()
+    arecv[t] = dot(values, wo[:, lanes_of(t)]).astype(BF16)
     finish_tp(4, arecv)
     attn = arecv[0].astype(F32)
     for s in range(1, T):
         attn = attn + arecv[s].astype(F32)
     aq[t] = attn.astype(BF16)
     attn = attn.astype(BF16).astype(F32)
-
-    def lanes_of(quarter):
-        return pl.ds(pl.multiple_of(quarter * Q, Q), Q)
 
     def row_sum(v):
         return jnp.sum(v, axis=1, keepdims=True)
@@ -595,7 +661,7 @@
         normed = mixed.astype(F32) * ffn_inverse * gains[1:2, lanes_of(quarter)]
         return mixed, normed.astype(BF16)
 
-    order = sorted(range(1, EP), key=lambda k: -k)
+    order = sorted(range(1, EP), key=lambda k: (-k.bit_length(), k ^ 1, k))
     far = EP // 2
     far_order, near_order = order[:far], order[far:]
 
@@ -665,7 +731,7 @@
         settle_recv(xr.at[t, k], d_recv.at[k])
         for j in range(1, pairs):
             remote(
-                xr.at[t, k], xr.at[t, k], x_send.at[0], x_recv.at[k, j], {"tp": quarter_at(j)}
+                xr.at[t, k], xr.at[t, k], x_send.at[0], x_recv.at[k - far, j - 1], {"tp": quarter_at(j)}
             ).start()
         to_sib(chunk_of[k], t, k)
     for k in near_order[::-1]:
@@ -674,7 +740,7 @@
     def relay_far(c):
         for k in members(c):
             for j in range(1, pairs):
-                settle_recv(xr.at[t, k], x_recv.at[k, j])
+                settle_recv(xr.at[t, k], x_recv.at[k - far, j - 1])
                 to_sib(c, lax.rem(t + T - 2 * j, T), k)
 
     def rows_of(blocks, c):
@@ -762,7 +828,11 @@
             for k in members(c):
                 xsend[j, k] = chip_sum(quarter, k).astype(BF16)
                 remote(
-                    xsend.at[j, k], xrecv.at[j, k], rx_send.at[0], rx_recv.at[k, j], {"tp": quarter}
+                    xsend.at[j, k],
+                    xrecv.at[j, k],
+                    rx_send.at[0],
+                    rx_recv.at[k - far, j - 1],
+                    {"tp": quarter},
                 ).start()
 
     def return_far(c):
@@ -771,7 +841,7 @@
         for k in members(c):
             total = chip_sum(t, k)
             for j in range(1, pairs):
-                settle_recv(xrecv.at[j, k], rx_recv.at[k, j])
+                settle_recv(xrecv.at[j, k], rx_recv.at[k - far, j - 1])
                 total = total + xrecv[j, k].astype(F32)
             rsend[0, k] = total.astype(BF16)
             remote(
@@ -818,8 +888,9 @@
     mixed_own = jnp.concatenate([mxrecv[s] for s in range(T)], axis=1).astype(F32)
     out_result[...] = (mixed_own + rms_scale(moe, gain(post_ffn_gain))).astype(BF16)[:R]
 
-    for phase, dst in sent_tp:
-        settle_send(dst.at[pl.ds(0, T - 1)], tp_send.at[phase])
+    fetch("out_result")
+    for slot, view in sorted(sent_tp.items()):
+        settle_send(view, tp_send.at[slot])
     settle_send(xr.at[0, pl.ds(0, far)], d_send.at[0])
     settle_send(xr.at[pl.ds(0, pairs), pl.ds(1, far - 1)], d_send.at[1])
     if pairs > 1:
@@ -830,6 +901,8 @@
     settle_send(part.at[pl.ds(0, pairs)], s1_send.at[0])
     settle_send(xr.at[0, pl.ds(0, far)], ret_send.at[0])
     settle_send(xr.at[pl.ds(0, pairs), pl.ds(1, far - 1)], ret_send.at[1])
+    for name in ("out_rope", "out_latent", "out_result"):
+        arrive(name)
 
 
 def hand_over(result, latent, rope, out_result, out_latent, out_rope):
@@ -906,9 +979,21 @@
             jax.ShapeDtypeStruct((R, C), BF16),
             jax.ShapeDtypeStruct((R, RD), BF16),
         ),
-        in_specs=[pl.BlockSpec(memory_space=pltpu.SMEM)] + [vm] * 8 + [hbm] * 13,
-        out_specs=(vm, vm, vm),
+        in_specs=[hbm] * 22,
+        out_specs=(hbm, hbm, hbm),
         scratch_shapes=[
+            pltpu.SMEM((R,), jnp.int32),
+            v(R, D),
+            v(D),
+            v(C),
+            v(D),
+            v(D),
+            v(D),
+            v(K, N, dtype=jnp.int32),
+            v(K, N, dtype=F32),
+            v(R, D),
+            v(R, C),
+            v(R, RD),
             v(*table.shape),
             v(R, SPAN, C),
             v(R, RD, SPAN),
@@ -929,8 +1014,10 @@
             v(RP, C, dtype=F32),
             v(RP, RD, dtype=F32),
             v(R, H, C),
-            v(2, T, R // 2 * LH, C),
-            v(2, T, R // 2 * LH, C),
+            v(T, SUB * LH, C),
+            v(T, SUB * LH, C),
+            v(T, (R - SUB) * LH, C),
+            v(T, (R - SUB) * LH, C),
             v(T, N, Q),
             v(T, N, Q),
             v(T, N, Q),
@@ -956,21 +1043,21 @@
             v(C * LH, KD, dtype=F32),
             v(R, H, SPAN, dtype=F32),
             v(R, H, SPAN),
+            dma((19,)),
+            dma((3,)),
             dma((10,)),
-            dma((9,)),
-            dma((9,)),
             dma((1,)),
             dma((pairs,)),
             dma((2,)),
             dma((EP,)),
             dma((1,)),
-            dma((EP, pairs)),
+            dma((far, max(1, pairs - 1))),
             dma((1,)),
             dma((len(chunks),)),
             dma((1,)),
             dma((len(chunks), pairs)),
             dma((1,)),
-            dma((EP, pairs)),
+            dma((far, max(1, pairs - 1))),
             dma((2,)),
             dma((2,)),
             pltpu.SemaphoreType.REGULAR((max(1, EP.bit_length() - 2),)),

time: 60.2 us -> 57.6 us (0.957)
  Pallas kernels: 59.3 us -> 56.8 us
    pallas_call x1, Pallas kernels: 57.8 us -> 55.3 us  [body(): pl.pallas_call(functools.partial(kernel, cfg), out_shape=(jax.ShapeDtypeS...]
where the time goes in v3:
time: 57.6 us; the launch traced here: 57.4 us
  Pallas kernels  56.8 us (99%)
  between operations  0.65 us (1%)
    pallas_call x1, Pallas kernels, body(): pl.pallas_call(functools.partial(kernel, cfg), out_shape=(jax.ShapeDtypeS...  55.3 us
    pallas_call x1, Pallas kernels, body(): pl.pallas_call(hand_over, out_shape=tuple((jax.ShapeDtypeStruct(o.shape,...  1.5 us

profile of v3, /device:TPU:0, one launch (start us, length us, event | category | flops | bytes accessed | tf_op | source)
XLA Modules:
  0.0 57.4 jit_solution(13953843144584884968)
XLA Ops:
  0.6 55.3 %shard_map.229 = (bf16[12,2048]{1,0:T(8,128)(2,1)}, bf16[12,512]{1,0:T(8,128)(2,1)}, bf16[12,64]{1,0:T(8,128)(2,1)}) custom-call(s32[12]{0:T(128)} %lengths_h.1, bf16[12,2048]{1,0:T(8,128)(2,1)} %tokens_h.1, bf16[2048]{0:T(1024)(128)(2,1)} %attn_gain_h.1, bf16[512]{0:T(512)(128)(2,1)} %latent_gain_h.1, bf16[2048]{0:T(1024)(128)(2,1)} %post_attn_gain_h.1, ...), custom_call_target="tpu_custom_call" | custom-call | tf_op jit(solution)/shard_map/pallas_call | solution.py:975
  55.9 1.5 %shard_map.230 = (bf16[12,2048]{1,0:T(8,128)(2,1)}, bf16[12,512]{1,0:T(8,128)(2,1)}, bf16[12,64]{1,0:T(8,128)(2,1)}) custom-call(bf16[12,2048]{1,0:T(8,128)(2,1)} %get-tuple-element.6.result, bf16[12,512]{1,0:T(8,128)(2,1)} %get-tuple-element.7.latent, bf16[12,64]{1,0:T(8,128)(2,1)} %get-tuple-element.8.rope), custom_call_target="tpu_custom_call" | custom-call | tf_op jit(solution)/shard_map/pallas_call | solution.py:1092

commit v4 on v3

--- a/solution.py
+++ b/solution.py
@@ -705,8 +705,6 @@
         _, normed = ffn_rows(*scaled_branch(aq[other].astype(F32), other), other)
         pack_slots(j, 0, normed)
         send_near(j)
-    mxsend[...] = dot(one_hot(6), mixed).astype(BF16).reshape(T, RP, Q)
-    scatter_tp(6, mxsend, mxrecv)
 
     chunk_of = {lo + k: c for c, (lo, n) in enumerate(chunks) for k in range(n)}
     far_chunks = range(1, len(chunks))
@@ -864,6 +862,8 @@
     experts(0)
     relay_far(1)
     return_near()
+    mxsend[...] = dot(one_hot(6), mixed).astype(BF16).reshape(T, RP, Q)
+    scatter_tp(6, mxsend, mxrecv)
     experts(1)
     reduce_far(1)
     return_far(1)

time: 57.6 us -> 57.6 us (level)
  no operation moved by 1% of the time
where the time goes in v4:
time: 57.6 us; the launch traced here: 57.4 us
  Pallas kernels  56.8 us (99%)
  between operations  0.65 us (1%)
    pallas_call x1, Pallas kernels, body(): pl.pallas_call(functools.partial(kernel, cfg), out_shape=(jax.ShapeDtypeS...  55.3 us
    pallas_call x1, Pallas kernels, body(): pl.pallas_call(hand_over, out_shape=tuple((jax.ShapeDtypeStruct(o.shape,...  1.5 us

profile of v4, /device:TPU:0, one launch (start us, length us, event | category | flops | bytes accessed | tf_op | source)
XLA Modules:
  0.0 57.4 jit_solution(12620237485398122958)
XLA Ops:
  0.6 55.3 %shard_map.229 = (bf16[12,2048]{1,0:T(8,128)(2,1)}, bf16[12,512]{1,0:T(8,128)(2,1)}, bf16[12,64]{1,0:T(8,128)(2,1)}) custom-call(s32[12]{0:T(128)} %lengths_h.1, bf16[12,2048]{1,0:T(8,128)(2,1)} %tokens_h.1, bf16[2048]{0:T(1024)(128)(2,1)} %attn_gain_h.1, bf16[512]{0:T(512)(128)(2,1)} %latent_gain_h.1, bf16[2048]{0:T(1024)(128)(2,1)} %post_attn_gain_h.1, ...), custom_call_target="tpu_custom_call" | custom-call | tf_op jit(solution)/shard_map/pallas_call | solution.py:975
  55.9 1.5 %shard_map.230 = (bf16[12,2048]{1,0:T(8,128)(2,1)}, bf16[12,512]{1,0:T(8,128)(2,1)}, bf16[12,64]{1,0:T(8,128)(2,1)}) custom-call(bf16[12,2048]{1,0:T(8,128)(2,1)} %get-tuple-element.6.result, bf16[12,512]{1,0:T(8,128)(2,1)} %get-tuple-element.7.latent, bf16[12,64]{1,0:T(8,128)(2,1)} %get-tuple-element.8.rope), custom_call_target="tpu_custom_call" | custom-call | tf_op jit(solution)/shard_map/pallas_call | solution.py:1092
